TPU v7x, 32 devices: a whole 2x2x4 slice. The times are simulated.
32 devices in a mesh: fs: 4 (over z), rep: 4 (over y, x), tp: 2 (over core).
Axes of the slice: x: 2, y: 2, z: 4, core: 2. Of those that a mesh axis runs over, the one named last changes fastest.
Arguments:
- inputs: bfloat16 [2048, 2048], P(('fs', 'rep')), may hold values from -6 to 6
- query_cot: bfloat16 [2048, 1024], P(('fs', 'rep'), 'tp'), may hold values from -0.125 to 0.125
- attended: bfloat16 [2048, 1024], P(('fs', 'rep')), may hold values from -6 to 6
- output_cot: bfloat16 [2048, 2048], P(('fs', 'rep'), 'tp'), may hold values from -0.125 to 0.125
- proj_query: bfloat16 [2048, 256], P('fs'), may hold values from -0.125 to 0.125
- proj_output: bfloat16 [1024, 256], P('fs'), may hold values from -0.1875 to 0.1875
- weight_query: float32 [2048, 1024], P('fs', 'tp'), may hold values from -0.125 to 0.125
- weight_output: float32 [1024, 2048], P('fs', 'tp'), may hold values from -0.1875 to 0.1875
- first_query: float32 [256, 1024], P('fs', 'tp'), may hold values from -6 to 6
- second_query: float32 [256, 1024], P('fs', 'tp'), may hold values from 0.0002 to 2
- first_output: float32 [256, 2048], P('fs', 'tp'), may hold values from -6 to 6
- second_output: float32 [256, 2048], P('fs', 'tp'), may hold values from 0.0002 to 2
Outputs:
- new_weight_query: float32 [2048, 1024], P('fs', 'tp')
- new_weight_output: float32 [1024, 2048], P('fs', 'tp')
- step_query: float32 [2048, 1024], P('fs', 'tp')
- step_output: float32 [1024, 2048], P('fs', 'tp')
- new_first_query: float32 [256, 1024], P('fs', 'tp')
- new_second_query: float32 [256, 1024], P('fs', 'tp')
- new_first_output: float32 [256, 2048], P('fs', 'tp')
- new_second_output: float32 [256, 2048], P('fs', 'tp')
- copy_query: bfloat16 [2048, 1024], P(None, 'tp')
- copy_output: bfloat16 [1024, 2048], P(None, 'tp')
All inputs are finite; a program needn't handle non-finite values.
Results may differ from a plain program's by a relative error of at most 0.0031.
Values may be sent and summed in bfloat16 or wider, within the bound.
No kernel may reach another device: no remote copies, remote signals or barrier semaphores. Data moves between devices by JAX's collectives and lax.ppermute only.
A program may use at most 64 MiB of HBM per device.

v0:
```python
import jax
import jax.numpy as jnp
from jax import lax
from jax.experimental import pallas as pl
from jax.experimental.pallas import tpu as pltpu
from jax.sharding import PartitionSpec as P

beta_first = 0.9
beta_second = 0.95
adam_eps = 1e-08
mean_eps = 1e-06
learn_rate = 0.02
code_scale = 2.0**17


f32 = jnp.float32
bf16 = jnp.bfloat16
VMEM = pl.BlockSpec(memory_space=pltpu.VMEM)
SMEM = pl.BlockSpec(memory_space=pltpu.SMEM)
ANY = pl.BlockSpec(memory_space=pl.ANY)
HBM = pl.BlockSpec(memory_space=pltpu.HBM)
TAIL = 16
MIB = 2**20


def moment_update(low_sum, first, second):
    first_new = beta_first * first + (1.0 - beta_first) * low_sum
    second_new = beta_second * second + (1.0 - beta_second) * low_sum * low_sum
    normed = first_new / (jnp.sqrt(second_new) + adam_eps)
    return (first_new, second_new, normed)


def contract_rows(left, right):
    return lax.dot_general(
        left,
        right,
        (((0,), (0,)), ((), ())),
        precision=lax.Precision.HIGHEST,
        preferred_element_type=f32,
    )


def local_general(inputs, query_cot, attended, output_cot, proj_query, proj_output, weight_query, weight_output, first_query, second_query, first_output, second_output):
    def gather(x):
        return lax.all_gather(x, "fs", axis=0, tiled=True)

    def low_of(acts, proj, cot):
        reduced = jnp.dot(acts, gather(proj), preferred_element_type=f32)
        part = contract_rows(reduced, cot.astype(f32))
        return lax.psum_scatter(part, "fs", scatter_dimension=0, tiled=True)

    low_query, low_output = lax.psum((low_of(inputs, proj_query, query_cot), low_of(attended, proj_output, output_cot)), "rep")
    first_q, second_q, normed_q = moment_update(low_query, first_query, second_query)
    first_o, second_o, normed_o = moment_update(low_output, first_output, second_output)
    total = lax.psum(jnp.sum(normed_q * normed_q) + jnp.sum(normed_o * normed_o), ("fs", "tp"))
    entries = (normed_q.size + normed_o.size) * lax.axis_size("fs") * lax.axis_size("tp")
    scale = lax.rsqrt(total / entries + mean_eps)
    step_q = scale * jnp.dot(proj_query, gather(normed_q.astype(bf16)), preferred_element_type=f32)
    step_o = scale * jnp.dot(proj_output, gather(normed_o.astype(bf16)), preferred_element_type=f32)
    new_q = weight_query - learn_rate * step_q
    new_o = weight_output - learn_rate * step_o
    return (new_q, new_o, step_q, step_o, first_q, second_q, first_o, second_o, gather(new_q.astype(bf16)), gather(new_o.astype(bf16)))


def fetch(pairs, sems):
    copies = [pltpu.make_async_copy(src, dst, sems.at[k]) for k, (src, dst) in enumerate(pairs)]
    for copy in copies:
        copy.start()
    for copy in copies:
        copy.wait()


def share_kernel(nr, place, proj_q, proj_o, out, sems):
    r, t = place[1], place[2]
    part_q, part_o, half = proj_q.shape[0] // nr, proj_o.shape[0] // nr, out.shape[1]
    mine = pl.ds(pl.multiple_of(t * half, half), half)
    fetch(
        [
            (proj_q.at[pl.ds(pl.multiple_of(r * part_q, part_q), part_q), mine], out.at[0:part_q, :]),
            (proj_o.at[pl.ds(pl.multiple_of(r * part_o, part_o), part_o), mine], out.at[part_q : part_q + part_o, :]),
        ],
        sems,
    )


def cot_kernel(nr, place, cot_q, cot_o, *rest):
    outs, sems = rest[:-1], rest[-1]
    r = place[1]
    block_q, block_o = cot_q.shape[1] // nr, cot_o.shape[1] // nr
    pairs = []
    for m, out in enumerate(outs):
        at = r ^ m
        pairs.append((cot_q.at[:, pl.ds(pl.multiple_of(at * block_q, block_q), block_q)], out.at[:, 0:block_q]))
        pairs.append((cot_o.at[:, pl.ds(pl.multiple_of(at * block_o, block_o), block_o)], out.at[:, block_q : block_q + block_o]))
    fetch(pairs, sems)


def cut_kernel(nr, place, weight_q, weight_o, out, sems):
    at = place[1] ^ (nr - 1)
    part_q, part_o = weight_q.shape[0] // nr, weight_o.shape[0] // nr
    cols = weight_q.shape[1]
    pairs = [(weight_q.at[pl.ds(pl.multiple_of(at * part_q, part_q), part_q), :], out.at[0:part_q, :])]
    for k in range(weight_o.shape[1] // cols):
        base = part_q + k * part_o
        rows = pl.ds(pl.multiple_of(at * part_o, part_o), part_o)
        pairs.append((weight_o.at[rows, k * cols : (k + 1) * cols], out.at[base : base + part_o, :]))
    fetch(pairs, sems)


def reduce_kernel(nf, nr, place, inputs, attended, proj_q, proj_o, own, *rest):
    near, (table, red) = rest[:-2], rest[-2:]
    f, r, t = place[0], place[1], place[2]
    half = table.shape[1]
    rows_q, rows_o = proj_q.shape[0], proj_o.shape[0]
    part_q, part_o = rows_q // nr, rows_o // nr
    part = part_q + part_o
    cut = nf * rows_q
    mine = pl.ds(pl.multiple_of(t * half, half), half)
    table[pl.ds(pl.multiple_of(f * rows_q, rows_q), rows_q), :] = proj_q[:, mine]
    table[pl.ds(pl.multiple_of(cut + f * rows_o, rows_o), rows_o), :] = proj_o[:, mine]
    for mr, ref in enumerate((own,) + near):
        for mz in range(1, nf):
            at = (f ^ mz) * nr + (r ^ mr)
            base = (mz - 1) * part
            table[pl.ds(pl.multiple_of(at * part_q, part_q), part_q), :] = ref[base : base + part_q, :]
            table[pl.ds(pl.multiple_of(cut + at * part_o, part_o), part_o), :] = ref[base + part_q : base + part, :]
    red_q = jnp.dot(inputs[...], table[0:cut, :], preferred_element_type=f32)
    red_o = jnp.dot(attended[...], table[cut:, :], preferred_element_type=f32)
    red[0:half, :] = red_q.T
    red[half : 2 * half, :] = red_o.T


def split_three(x):
    high = x.astype(bf16)
    rest = x - high.astype(f32)
    mid = rest.astype(bf16)
    return high, mid, (rest - mid.astype(f32)).astype(bf16)


def low_kernel(nf, nr, block_q, place, *refs):
    cots, mine, other, outs, low = refs[:nr], refs[nr : 2 * nr], refs[2 * nr : 3 * nr], refs[3 * nr : 3 * nr + nf], refs[-1]
    f, t = place[0], place[2]
    half = mine[0].shape[0] // 2
    cot = jnp.concatenate([c[...] for c in cots], axis=0)
    for which, group in enumerate((mine, other)):
        top = pl.multiple_of((t ^ which) * half, half)
        for k, (lo, hi) in enumerate(((0, block_q), (block_q, cot.shape[1]))):
            left = jnp.concatenate([g[k * half : (k + 1) * half, :] for g in group], axis=1)
            acc = None
            for term in split_three(left):
                got = jnp.dot(term, cot[:, lo:hi], preferred_element_type=f32)
                acc = got if acc is None else acc + got
            low[pl.ds(top, half), lo:hi] = acc
    rows = low.shape[0] // nf
    for m in range(nf):
        outs[m][...] = low[pl.ds(pl.multiple_of((f ^ m) * rows, rows), rows), :]


def pack_total(spread):
    row = lax.broadcasted_iota(jnp.int32, spread.shape, 0)
    high, mid, last = (x.astype(f32) for x in split_three(spread))
    packed = jnp.where(row == 0, high, jnp.where(row == 1, mid, jnp.where(row == 2, last, 0.0)))
    return jnp.concatenate([packed, jnp.zeros_like(packed)], axis=0).astype(bf16)


def add_totals(tails):
    acc = tails[0].astype(f32)
    for tail in tails[1:]:
        acc = acc + tail.astype(f32)
    return jnp.sum(acc, axis=0, keepdims=True)


def moment_kernel(nf, block_q, place, *refs):
    parts, (first_q, second_q, first_o, second_o, low_out, half_out) = refs[:nf], refs[nf:]
    r = place[1]
    low = parts[0][...]
    for p in parts[1:]:
        low = low + p[...]
    low_out[...] = low
    block_o = low.shape[1] - block_q
    rows = low.shape[0]
    total = jnp.zeros((), f32)
    for first, second, lo, width in ((first_q, second_q, 0, block_q), (first_o, second_o, block_q, block_o)):
        cols = pl.ds(pl.multiple_of(r * width, width), width)
        _, _, normed = moment_update(low[:, lo : lo + width], first[:, cols], second[:, cols])
        half_out[0:rows, lo : lo + width] = normed.astype(bf16)
        total = total + jnp.sum(normed * normed)
    half_out[rows : rows + TAIL, :] = pack_total(jnp.full((8, low.shape[1]), total, f32))


def line_kernel(nf, place, *refs):
    blocks, (table, total) = refs[:nf], refs[nf:]
    f = place[0]
    rows = blocks[0].shape[0] - TAIL
    for m, block in enumerate(blocks):
        table[pl.ds(pl.multiple_of((f ^ m) * rows, rows), rows), :] = block[0:rows, :]
    found = add_totals([block[rows : rows + TAIL, 0 : total.shape[1]] for block in blocks])
    total[...] = jnp.broadcast_to(found, total.shape)


def left_kernel(place, mine, other, out):
    t = place[2]
    half = mine.shape[1]
    out[:, pl.ds(pl.multiple_of(t * half, half), half)] = mine[...]
    out[:, pl.ds(pl.multiple_of((1 - t) * half, half), half)] = other[...]


def step_kernel(nf, nr, block_q, count, place, left, *rest):
    halves, totals, lows, rest = rest[:nr], rest[nr : 2 * nr], rest[2 * nr : 3 * nr], rest[3 * nr :]
    codes, near, rest = rest[: nr - 1], rest[nr - 1], rest[nr:]
    first_q, second_q, first_o, second_o, weight_q, weight_o = rest[:6]
    copy_q, copy_o, new_q, new_o, step_q, step_o, new_fq, new_sq, new_fo, new_so, table, scale_out = rest[6:18]
    made_q, made_o, fresh_q, fresh_o, moved_q, moved_o, got_q, got_o, made_fq, made_sq, made_fo, made_so, sems = rest[18:]
    f, r = place[0], place[1]
    rows_q, cols_q = weight_q.shape
    rows_o, cols_o = weight_o.shape
    part_q, part_o = rows_q // nr, rows_o // nr
    cut = nf * rows_q
    block_o = cols_o // nr
    total = totals[0][...]
    for x in totals[1:]:
        total = total + x[...]
    scale = lax.rsqrt(total / count + mean_eps)
    scale_out[...] = scale
    scale = scale[0:1, 0:1]

    for m in range(nr):
        at = r ^ m
        table[:, pl.ds(pl.multiple_of(at * block_q, block_q), block_q)] = halves[m][:, 0:block_q]
        table[:, pl.ds(pl.multiple_of(cols_q + at * block_o, block_o), block_o)] = halves[m][:, block_q:]

    pending = []

    def send(src, dst):
        copy = pltpu.make_async_copy(src, dst, sems.at[len(pending)])
        copy.start()
        pending.append(copy)

    for mz in range(nf):
        at_q = pl.ds(pl.multiple_of((f ^ mz) * rows_q, rows_q), rows_q)
        at_o = pl.ds(pl.multiple_of((f ^ mz) * rows_o, rows_o), rows_o)
        left_o = pl.ds(pl.multiple_of(cut + (f ^ mz) * rows_o, rows_o), rows_o)
        found_q = scale * jnp.dot(left[at_q, :], table[:, 0:cols_q], preferred_element_type=f32)
        if mz == 0:
            moved_q[...] = found_q
            fresh_q[...] = weight_q[...] - learn_rate * found_q
            made_q[at_q, :] = fresh_q[...].astype(bf16)
            send(moved_q, step_q)
            send(fresh_q, new_q)
            send(made_q.at[at_q, :], copy_q.at[at_q, :])
        else:
            got_q[...] = found_q
            for mr in range(nr if mz == 1 else nr - 1):
                at = (r ^ mr) * part_q
                old = codes[mr][mz - 1, 0:part_q, :] if mr < nr - 1 else near[0:part_q, :]
                to = pl.ds(pl.multiple_of((f ^ mz) * rows_q + at, part_q), part_q)
                made_q[to, :] = (old - learn_rate * got_q[pl.ds(pl.multiple_of(at, part_q), part_q), :]).astype(bf16)
                send(made_q.at[to, :], copy_q.at[to, :])
        found_o = scale * jnp.dot(left[left_o, :], table[:, cols_q:], preferred_element_type=f32)
        if mz == 0:
            moved_o[...] = found_o
            fresh_o[...] = weight_o[...] - learn_rate * found_o
            made_o[at_o, :] = fresh_o[...].astype(bf16)
            send(moved_o, step_o)
            send(fresh_o, new_o)
            send(made_o.at[at_o, :], copy_o.at[at_o, :])
        else:
            got_o[...] = found_o
            for mr in range(nr if mz == 1 else nr - 1):
                at = (r ^ mr) * part_o
                to = pl.ds(pl.multiple_of((f ^ mz) * rows_o + at, part_o), part_o)
                for k in range(cols_o // cols_q):
                    base = part_q + k * part_o
                    lo = k * cols_q
                    old = codes[mr][mz - 1, base : base + part_o, :] if mr < nr - 1 else near[base : base + part_o, :]
                    made_o[to, lo : lo + cols_q] = (
                        old - learn_rate * got_o[pl.ds(pl.multiple_of(at, part_o), part_o), lo : lo + cols_q]
                    ).astype(bf16)
                send(made_o.at[to, :], copy_o.at[to, :])
    for first, second, made_f, made_s, new_f, new_s, lo, width in (
        (first_q, second_q, made_fq, made_sq, new_fq, new_sq, 0, block_q),
        (first_o, second_o, made_fo, made_so, new_fo, new_so, block_q, block_o),
    ):
        for m in range(nr):
            cols = pl.ds(pl.multiple_of((r ^ m) * width, width), width)
            first_new, second_new, _ = moment_update(lows[m][:, lo : lo + width], first[:, cols], second[:, cols])
            made_f[:, cols] = first_new
            made_s[:, cols] = second_new
        send(made_f, new_f)
        send(made_s, new_s)
    for copy in pending:
        copy.wait()


def corner_kernel(nf, nr, place, left, table, scale, tops, ends, had_q, had_o, copy_q, copy_o, made_q, made_o, sems):
    f, r = place[0], place[1]
    scale = scale[0:1, 0:1]
    cols_q = copy_q.shape[1]
    cols_o = copy_o.shape[1]
    part_q = made_q.shape[0] // (nf - 2)
    part_o = made_o.shape[0] // (nf - 2)
    cut = nf * nr * part_q
    pending = []
    for k, mz in enumerate(range(2, nf)):
        at = (f ^ mz) * nr + (r ^ (nr - 1))
        to_q = pl.ds(pl.multiple_of(at * part_q, part_q), part_q)
        to_o = pl.ds(pl.multiple_of(at * part_o, part_o), part_o)
        got = scale * jnp.dot(left[to_q, :], table[:, 0:cols_q], preferred_element_type=f32)
        here_q = pl.ds(k * part_q, part_q)
        made_q[here_q, :] = (tops[here_q, :] - learn_rate * got).astype(bf16)
        copy = pltpu.make_async_copy(made_q.at[here_q, :], copy_q.at[to_q, :], sems.at[2 * k])
        copy.start()
        pending.append(copy)
        from_o = pl.ds(pl.multiple_of(cut + at * part_o, part_o), part_o)
        got = scale * jnp.dot(left[from_o, :], table[:, cols_q:], preferred_element_type=f32)
        here_o = pl.ds(k * part_o, part_o)
        for c in range(cols_o // cols_q):
            old = ends[pl.ds(k * part_q + c * part_o, part_o), :]
            lo = c * cols_q
            made_o[here_o, lo : lo + cols_q] = (old - learn_rate * got[:, lo : lo + cols_q]).astype(bf16)
        copy = pltpu.make_async_copy(made_o.at[here_o, :], copy_o.at[to_o, :], sems.at[2 * k + 1])
        copy.start()
        pending.append(copy)
    for copy in pending:
        copy.wait()


def shape(x, dtype=f32):
    return jax.ShapeDtypeStruct(tuple(x), dtype)


def call(kernel, outs, args, scratch=(), limit=6 * MIB, places=VMEM, source=VMEM):
    many = isinstance(outs, list)
    return pl.pallas_call(
        kernel,
        out_shape=outs,
        in_specs=[SMEM] + [source] * (len(args) - 1),
        out_specs=[places] * len(outs) if many else places,
        scratch_shapes=scratch,
        compiler_params=pltpu.CompilerParams(vmem_limit_bytes=limit),
    )(*args)


def local_short(nf, nr, inputs, query_cot, attended, output_cot, proj_query, proj_output, weight_query, weight_output, first_query, second_query, first_output, second_output):
    f, r, t = (lax.axis_index(a) for a in ("fs", "rep", "tp"))
    place = jnp.stack([f, r, t]).astype(jnp.int32)
    hold = lax.optimization_barrier

    def swap(x, axis, m, n):
        return lax.ppermute(x, axis, [(i, i ^ m) for i in range(n)])

    fs_order = list(range(nf - 1, 0, -1))
    rep_order = list(range(nr - 1, 0, -1))

    def over_fs(make):
        got = {m: swap(make(m), "fs", m, nf) for m in fs_order}
        return [got[m] for m in range(1, nf)]

    def over_rep(make):
        got = {m: swap(make(m), "rep", m, nr) for m in rep_order}
        return [got[m] for m in range(1, nr)]

    def over_tp(x):
        return swap(x, "tp", 1, 2)

    tokens = inputs.shape[0]
    rank = proj_query.shape[1]
    half = rank // 2
    rows_q, rows_o = proj_query.shape[0], proj_output.shape[0]
    part_q, part_o = rows_q // nr, rows_o // nr
    cols_q, cols_o = query_cot.shape[1], output_cot.shape[1]
    block_q, block_o = cols_q // nr, cols_o // nr
    block = block_q + block_o
    rows = rank // nf

    share = call(
        lambda *a: share_kernel(nr, *a),
        shape((part_q + part_o, half), bf16),
        (place, proj_query, proj_output),
        scratch=[pltpu.SemaphoreType.DMA((2,))],
        source=ANY,
    )
    far = over_fs(lambda m: share)

    def encode(at, old_q, old_o):
        parts = [lax.dynamic_slice(old_q, (at * part_q, 0), (part_q, cols_q))]
        for k in range(cols_o // cols_q):
            parts.append(lax.dynamic_slice(old_o, (at * part_o, k * cols_q), (part_o, cols_q)))
        return (jnp.concatenate(parts, axis=0) * code_scale).astype(jnp.float16)

    code = encode(r, weight_query, weight_output)
    code_far = {m: swap(code, "fs", m, nf) for m in range(1, nf)}

    cots = call(
        lambda *a: cot_kernel(nr, *a),
        [shape((tokens, block), bf16)] * nr,
        (place, query_cot, output_cot),
        scratch=[pltpu.SemaphoreType.DMA((2 * nr,))],
        source=ANY,
    )
    cots = [cots[0]] + over_rep(lambda m: cots[m])

    corner = call(
        lambda *a: cut_kernel(nr, *a),
        shape(code.shape),
        (place, weight_query, weight_output),
        scratch=[pltpu.SemaphoreType.DMA((1 + cols_o // cols_q,))],
        source=ANY,
    )
    corner = (corner * code_scale).astype(jnp.float16)
    corners = {1: swap(corner, "fs", 1, nf)}

    own = jnp.concatenate(far, axis=0)
    near = over_rep(lambda m: own)

    table, red = call(
        lambda *a: reduce_kernel(nf, nr, *a),
        [shape(((rows_q + rows_o) * nf, half), bf16), shape((2 * half, tokens))],
        (place, inputs, attended, proj_query, proj_output, own, *near),
    )
    mine = [red] + over_rep(lambda m: red)
    other = [over_tp(x) for x in mine]
    parts = call(
        lambda *a: low_kernel(nf, nr, block_q, *a),
        [shape((rows, block))] * nf,
        (place, *cots, *mine, *other),
        scratch=[pltpu.VMEM((rank, block), f32)],
    )
    got = over_fs(lambda m: parts[m])

    def spread(piece):
        return swap(piece, "rep", 1, nr), swap(piece, "rep", 2, nr)

    later = hold((parts[0], *(code_far[m] for m in range(2, nf))))[1:]
    pieces = {1: code_far[1], **dict(zip(range(2, nf), later))}
    pairs = {m: spread(pieces[m]) for m in range(1, nf)}
    tops = swap(jnp.concatenate([pairs[m][0][:part_q] for m in range(2, nf)], axis=0), "rep", 2, nr)
    ends = swap(jnp.concatenate([pairs[m][1][part_q:] for m in range(2, nf)], axis=0), "rep", 1, nr)

    moments = (first_query, second_query, first_output, second_output)
    low, half_block = call(
        lambda *a: moment_kernel(nf, block_q, *a),
        [shape((rows, block)), shape((rows + TAIL, block), bf16)],
        (place, parts[0], *got, *moments),
    )
    half_far = over_fs(lambda m: half_block)
    other_table = over_tp(table)
    left = call(left_kernel, shape(((rows_q + rows_o) * nf, rank), bf16), (place, table, other_table))
    half_own, line = call(
        lambda *a: line_kernel(nf, *a), [shape((rank, block), bf16), shape((8, 128))], (place, half_block, *half_far)
    )
    halves = [half_own] + over_rep(lambda m: half_own)
    line = line + over_tp(line)
    totals = [line] + over_rep(lambda m: line)
    lows = [low] + over_rep(lambda m: low)
    near = hold((pieces[1], *pairs[1], corners[1], half_own))[:-1]
    pieces[1], pairs[1], corners[1] = near[0], near[1:3], near[3]

    def decode(x):
        return x.astype(f32) * (1.0 / code_scale)

    groups = ([pieces[m], *pairs[m]] for m in range(1, nf))
    codes = [decode(jnp.stack(x)) for x in zip(*groups)]
    count = rank * (cols_q + cols_o) * 2
    copy_q, copy_o, new_q, new_o, step_q, step_o, *new_state, all_half, scale = pl.pallas_call(
        lambda *a: step_kernel(nf, nr, block_q, count, *a),
        out_shape=[
            shape((rows_q * nf, cols_q), bf16),
            shape((rows_o * nf, cols_o), bf16),
            shape((rows_q, cols_q)),
            shape((rows_o, cols_o)),
            shape((rows_q, cols_q)),
            shape((rows_o, cols_o)),
            *[shape((rows, cols_q))] * 2,
            *[shape((rows, cols_o))] * 2,
            shape((rank, cols_q + cols_o), bf16),
            shape((8, 128)),
        ],
        in_specs=[SMEM] + [VMEM] * (4 * nr + 7),
        out_specs=[ANY] * 10 + [VMEM] * 2,
        scratch_shapes=[
            pltpu.VMEM((rows_q * nf, cols_q), bf16),
            pltpu.VMEM((rows_o * nf, cols_o), bf16),
            pltpu.VMEM((rows_q, cols_q), f32),
            pltpu.VMEM((rows_o, cols_o), f32),
            pltpu.VMEM((rows_q, cols_q), f32),
            pltpu.VMEM((rows_o, cols_o), f32),
            pltpu.VMEM((rows_q, cols_q), f32),
            pltpu.VMEM((rows_o, cols_o), f32),
            *[pltpu.VMEM((rows, cols_q), f32)] * 2,
            *[pltpu.VMEM((rows, cols_o), f32)] * 2,
            pltpu.SemaphoreType.DMA((10 + 2 * nr * (nf - 1),)),
        ],
        name="step",
        compiler_params=pltpu.CompilerParams(vmem_limit_bytes=24 * MIB),
    )(place, left, *halves, *totals, *lows, *codes, decode(corners[1]), *moments, weight_query, weight_output)
    tops, ends = hold((tops, ends, scale))[:2]
    copy_q, copy_o = pl.pallas_call(
        lambda *a: corner_kernel(nf, nr, *a),
        out_shape=[shape(copy_q.shape, bf16), shape(copy_o.shape, bf16)],
        in_specs=[SMEM] + [VMEM] * 5 + [ANY] * 2,
        out_specs=[ANY] * 2,
        scratch_shapes=[
            pltpu.VMEM(((nf - 2) * part_q, cols_q), bf16),
            pltpu.VMEM(((nf - 2) * part_o, cols_o), bf16),
            pltpu.SemaphoreType.DMA((2 * (nf - 2),)),
        ],
        input_output_aliases={6: 0, 7: 1},
        name="corner",
        compiler_params=pltpu.CompilerParams(vmem_limit_bytes=6 * MIB),
    )(place, left, all_half, scale, decode(tops), decode(ends), copy_q, copy_o)
    return (new_q, new_o, step_q, step_o, *new_state, copy_q, copy_o)


def solution(mesh):
    nf, nr, nt = (mesh.shape[a] for a in ("fs", "rep", "tp"))

    def local(*args):
        rows_o = args[5].shape[0]
        rank = args[4].shape[1]
        if nt == 2 and nf == 4 and nr == 4 and rows_o % (16 * nr) == 0 and rank % 256 == 0:
            return local_short(nf, nr, *args)
        return local_general(*args)

    spec = P("fs", "tp")
    return jax.shard_map(
        local,
        mesh=mesh,
        in_specs=(
            P(("fs", "rep"), None),
            P(("fs", "rep"), "tp"),
            P(("fs", "rep"), None),
            P(("fs", "rep"), "tp"),
            P("fs", None),
            P("fs", None),
        )
        + (spec,) * 6,
        out_specs=(spec,) * 8 + (P(None, "tp"), P(None, "tp")),
        check_vma=False,
    )
```

profile of v0, /device:TPU:0, one launch (start us, length us, event | category | flops | bytes accessed | tf_op | source)
XLA Modules:
  0.0 131.6 jit_solution(6227551964242167242)
XLA Ops:
  3.3 3.1 %collective-permute-start = (bf16[192,128]{1,0:T(8,128)(2,1)S(1)}, bf16[192,128]{1,0:T(8,128)(2,1)S(1)}, u32[]{:S(2)}, u32[]{:S(2)}) collective-permute-start(bf16[192,128]{1,0:T(8,128)(2,1)S(1)} %shard_map.195), channel_id=1, source_target_pairs={{0,8},{8,0},{16,24},{24,16},{1,9},{9,1},{17,25},{25,17},{2,10},{10... | collective-permute-start | bytes 147464 | tf_op jit(solution)/shard_map/ppermute | solution.py:350
  6.4 2.5 %collective-permute-start.2 = (bf16[192,128]{1,0:T(8,128)(2,1)S(1)}, bf16[192,128]{1,0:T(8,128)(2,1)S(1)}, u32[]{:S(2)}, u32[]{:S(2)}) collective-permute-start(bf16[192,128]{1,0:T(8,128)(2,1)S(1)} %shard_map.195), channel_id=1, source_target_pairs={{0,24},{8,16},{16,8},{24,0},{1,25},{9,17},{17,9},{25,1},{2,26},{10... | collective-permute-start | bytes 147464 | tf_op jit(solution)/shard_map/ppermute | solution.py:350
  14.4 1.5 %collective-permute-start.8 = (bf16[128,384]{1,0:T(8,128)(2,1)}, bf16[128,384]{1,0:T(8,128)(2,1)}, u32[]{:S(2)}, u32[]{:S(2)}) collective-permute-start(bf16[128,384]{1,0:T(8,128)(2,1)} %get-tuple-element.49), channel_id=1, source_target_pairs={{0,4},{2,6},{4,0},{6,2},{1,5},{3,7},{5,1},{7,3},{8,12},{10,14},{12... | collective-permute-start | bytes 294920 | tf_op jit(solution)/shard_map/ppermute | solution.py:350
  19.5 1.7 %constant_dynamic-slice_fusion.1 = f32[128,512]{1,0:T(8,128)} fusion(f32[512,512]{1,0:T(8,128)} %a_22_.1, s32[]{:T(128)S(6)} %select_n.7), kind=kLoop, calls=%fused_computation.16 | loop fusion | bytes 524292 | tf_op jit(solution)/shard_map/dynamic_slice | solution.py:386
  21.2 2.2 %collective-permute-done.5.a_8_ = bf16[576,128]{1,0:T(8,128)(2,1)S(1)} collective-permute-done((bf16[576,128]{1,0:T(8,128)(2,1)S(1)}, bf16[576,128]{1,0:T(8,128)(2,1)S(1)}, u32[]{:S(2)}, u32[]{:S(2)}) %collective-permute-start.5) | collective-permute-done | bytes 147488 | tf_op jit(solution)/shard_map/ppermute | solution.py:350
  23.4 1.8 %collective-permute-done.4.a_7_ = bf16[576,128]{1,0:T(8,128)(2,1)S(1)} collective-permute-done((bf16[576,128]{1,0:T(8,128)(2,1)S(1)}, bf16[576,128]{1,0:T(8,128)(2,1)S(1)}, u32[]{:S(2)}, u32[]{:S(2)}) %collective-permute-start.4) | collective-permute-done | bytes 147488 | tf_op jit(solution)/shard_map/ppermute | solution.py:350
  34.7 4.4 %collective-permute-done.9.a_4_ = bf16[128,384]{1,0:T(8,128)(2,1)S(1)} collective-permute-done((bf16[128,384]{1,0:T(8,128)(2,1)S(1)}, bf16[128,384]{1,0:T(8,128)(2,1)S(1)}, u32[]{:S(2)}, u32[]{:S(2)}) %collective-permute-start.9) | collective-permute-done | bytes 98336 | tf_op jit(solution)/shard_map/ppermute | solution.py:350
  40.8 2.7 %collective-permute-start.38 = (f16[256,512]{1,0:T(8,128)(2,1)S(1)}, f16[256,512]{1,0:T(8,128)(2,1)S(1)}, u32[]{:S(2)}, u32[]{:S(2)}) collective-permute-start(f16[256,512]{1,0:T(8,128)(2,1)S(1)} %fusion), channel_id=1, source_target_pairs={{0,24},{8,16},{16,8},{24,0},{1,25},{9,17},{17,9},{25,1},{2,26},{10... | collective-permute-start | bytes 786440 | tf_op jit(solution)/shard_map/ppermute | solution.py:350
  43.5 1.6 %shard_map.199 = (f32[64,384]{1,0:T(8,128)S(1)}, f32[64,384]{1,0:T(8,128)S(1)}, f32[64,384]{1,0:T(8,128)S(1)}, f32[64,384]{1,0:T(8,128)S(1)}) custom-call(s32[3]{0:T(128)S(1)} %copy-done.16, bf16[128,384]{1,0:T(8,128)(2,1)S(1)} %get-tuple-element.47.a_1_, bf16[128,384]{1,0:T(8,128)(2,1)} %collective-permute-done.7.a_2_, ...), custom_call_target="tpu_custom_call" | custom-call | tf_op jit(solution)/shard_map/pallas_call | solution.py:334
  45.1 1.8 %collective-permute-start.17 = (f32[64,384]{1,0:T(8,128)S(1)}, f32[64,384]{1,0:T(8,128)S(1)}, u32[]{:S(2)}, u32[]{:S(2)}) collective-permute-start(f32[64,384]{1,0:T(8,128)S(1)} %get-tuple-element.53), channel_id=1, source_target_pairs={{0,8},{8,0},{16,24},{24,16},{1,9},{9,1},{17,25},{25,17},{2,10},{10... | collective-permute-start | bytes 294920 | tf_op jit(solution)/shard_map/ppermute | solution.py:350
  49.6 8.4 %collective-permute-done.17.a_2_ = f32[64,384]{1,0:T(8,128)S(1)} collective-permute-done((f32[64,384]{1,0:T(8,128)S(1)}, f32[64,384]{1,0:T(8,128)S(1)}, u32[]{:S(2)}, u32[]{:S(2)}) %collective-permute-start.17) | collective-permute-done | bytes 98336 | tf_op jit(solution)/shard_map/ppermute | solution.py:350
  58.0 2.5 %collective-permute-start.36 = (f16[256,512]{1,0:T(8,128)(2,1)S(1)}, f16[256,512]{1,0:T(8,128)(2,1)S(1)}, u32[]{:S(2)}, u32[]{:S(2)}) collective-permute-start(f16[256,512]{1,0:T(8,128)(2,1)S(1)} %multiply_convert_fusion), channel_id=1, source_target_pairs={{0,8},{8,0},{16,24},{24,16},{1,9},{9,1},{17,25},{25,17},{2,10},{10... | collective-permute-start | bytes 786440 | tf_op jit(solution)/shard_map/ppermute | solution.py:350
  60.5 13.2 %collective-permute-done.18.a_3_ = f32[64,384]{1,0:T(8,128)S(1)} collective-permute-done((f32[64,384]{1,0:T(8,128)S(1)}, f32[64,384]{1,0:T(8,128)S(1)}, u32[]{:S(2)}, u32[]{:S(2)}) %collective-permute-start.18) | collective-permute-done | bytes 98336 | tf_op jit(solution)/shard_map/ppermute | solution.py:350
  76.5 2.5 %collective-permute-start.22 = (bf16[80,384]{1,0:T(8,128)(2,1)S(1)}, bf16[80,384]{1,0:T(8,128)(2,1)S(1)}, u32[]{:S(2)}, u32[]{:S(2)}) collective-permute-start(bf16[80,384]{1,0:T(8,128)(2,1)S(1)} %get-tuple-element.56.a_1_), channel_id=1, source_target_pairs={{0,24},{8,16},{16,8},{24,0},{1,25},{9,17},{17,9},{25,1},{2,26},{10... | collective-permute-start | bytes 184328 | tf_op jit(solution)/shard_map/ppermute | solution.py:350
  79.0 3.5 %collective-permute-done.22.a_4_ = bf16[80,384]{1,0:T(8,128)(2,1)S(1)} collective-permute-done((bf16[80,384]{1,0:T(8,128)(2,1)S(1)}, bf16[80,384]{1,0:T(8,128)(2,1)S(1)}, u32[]{:S(2)}, u32[]{:S(2)}) %collective-permute-start.22) | collective-permute-done | bytes 61472 | tf_op jit(solution)/shard_map/ppermute | solution.py:350
  82.8 5.2 %collective-permute-done.21.a_3_ = bf16[80,384]{1,0:T(8,128)(2,1)S(1)} collective-permute-done((bf16[80,384]{1,0:T(8,128)(2,1)S(1)}, bf16[80,384]{1,0:T(8,128)(2,1)S(1)}, u32[]{:S(2)}, u32[]{:S(2)}) %collective-permute-start.21) | collective-permute-done | bytes 61472 | tf_op jit(solution)/shard_map/ppermute | solution.py:350
  88.0 4.2 %collective-permute-done.20.a_2_ = bf16[80,384]{1,0:T(8,128)(2,1)S(1)} collective-permute-done((bf16[80,384]{1,0:T(8,128)(2,1)S(1)}, bf16[80,384]{1,0:T(8,128)(2,1)S(1)}, u32[]{:S(2)}, u32[]{:S(2)}) %collective-permute-start.20) | collective-permute-done | bytes 61472 | tf_op jit(solution)/shard_map/ppermute | solution.py:350
  104.4 2.4 %collective-permute-done.40 = f16[256,512]{1,0:T(8,128)(2,1)S(1)} collective-permute-done((f16[256,512]{1,0:T(8,128)(2,1)S(1)}, f16[256,512]{1,0:T(8,128)(2,1)S(1)}, u32[]{:S(2)}, u32[]{:S(2)}) %collective-permute-start.40) | collective-permute-done | bytes 262176 | tf_op jit(solution)/shard_map/ppermute | solution.py:350
  109.5 3.0 %collective-permute-done.27.a_7_ = f32[8,128]{1,0:T(8,128)S(1)} collective-permute-done((f32[8,128]{1,0:T(8,128)S(1)}, f32[8,128]{1,0:T(8,128)S(1)}, u32[]{:S(2)}, u32[]{:S(2)}) %collective-permute-start.27) | collective-permute-done | bytes 4128 | tf_op jit(solution)/shard_map/ppermute | solution.py:350
  112.4 1.6 %collective-permute-start.25 = (bf16[256,384]{1,0:T(8,128)(2,1)S(1)}, bf16[256,384]{1,0:T(8,128)(2,1)S(1)}, u32[]{:S(2)}, u32[]{:S(2)}) collective-permute-start(bf16[256,384]{1,0:T(8,128)(2,1)S(1)} %get-tuple-element.57.a_2_), channel_id=1, source_target_pairs={{0,6},{2,4},{4,2},{6,0},{1,7},{3,5},{5,3},{7,1},{8,14},{10,12},{12... | collective-permute-start | bytes 589832 | tf_op jit(solution)/shard_map/ppermute | solution.py:350
  119.4 1.7 %collective-permute-done.25.a_5_ = bf16[256,384]{1,0:T(8,128)(2,1)S(1)} collective-permute-done((bf16[256,384]{1,0:T(8,128)(2,1)S(1)}, bf16[256,384]{1,0:T(8,128)(2,1)S(1)}, u32[]{:S(2)}, u32[]{:S(2)}) %collective-permute-start.25) | collective-permute-done | bytes 196640 | tf_op jit(solution)/shard_map/ppermute | solution.py:350
  121.1 2.4 %collective-permute-done.24.a_4_ = bf16[256,384]{1,0:T(8,128)(2,1)S(1)} collective-permute-done((bf16[256,384]{1,0:T(8,128)(2,1)S(1)}, bf16[256,384]{1,0:T(8,128)(2,1)S(1)}, u32[]{:S(2)}, u32[]{:S(2)}) %collective-permute-start.24) | collective-permute-done | bytes 196640 | tf_op jit(solution)/shard_map/ppermute | solution.py:350
  124.9 4.9 %step.1 = (bf16[2048,512]{1,0:T(8,128)(2,1)}, bf16[1024,1024]{1,0:T(8,128)(2,1)}, f32[512,512]{1,0:T(8,128)}, f32[256,1024]{1,0:T(8,128)}, f32[512,512]{1,0:T(8,...) custom-call(s32[3]{0:T(128)S(1)} %copy-done.16, ...), custom_call_target="tpu_custom_call" | custom-call | tf_op jit(solution)/shard_map/step/pallas_call | solution.py:465
  129.9 1.6 %corner.1 = (bf16[2048,512]{1,0:T(8,128)(2,1)}, bf16[1024,1024]{1,0:T(8,128)(2,1)}) custom-call(s32[3]{0:T(128)S(1)} %copy-done.16, bf16[3072,256]{1,0:T(8,128)(2,1)S(1)} %shard_map.197.a_1_, bf16[256,1536]{1,0:T(8,128)(2,1)S(1)} %get-tuple-element.74.a_2_, f32[8,128]{1,0:T(8,128)S(1)} %get-tuple-element.75.a_3_, ...), custom_call_target="tpu_custom_call", output_to_operand_aliasing={{0}: (6, {}), {1}: (7, {})} | custom-call | tf_op jit(solution)/shard_map/corner/pallas_call | solution.py:498
  (136 shorter events, 50.0 us)
Async XLA Ops:
  3.3 12.6 %collective-permute-start = (bf16[192,128]{1,0:T(8,128)(2,1)S(1)}, bf16[192,128]{1,0:T(8,128)(2,1)S(1)}, u32[]{:S(2)}, u32[]{:S(2)}) collective-permute-start(bf16[192,128]{1,0:T(8,128)(2,1)S(1)} %shard_map.195), channel_id=1, source_target_pairs={{0,8},{8,0},{16,24},{24,16},{1,9},{9,1},{17,25},{25,17},{2,10},{10... | collective-permute-start | bytes 147464 | tf_op jit(solution)/shard_map/ppermute | solution.py:350
  6.4 9.5 %collective-permute-start.2 = (bf16[192,128]{1,0:T(8,128)(2,1)S(1)}, bf16[192,128]{1,0:T(8,128)(2,1)S(1)}, u32[]{:S(2)}, u32[]{:S(2)}) collective-permute-start(bf16[192,128]{1,0:T(8,128)(2,1)S(1)} %shard_map.195), channel_id=1, source_target_pairs={{0,24},{8,16},{16,8},{24,0},{1,25},{9,17},{17,9},{25,1},{2,26},{10... | collective-permute-start | bytes 147464 | tf_op jit(solution)/shard_map/ppermute | solution.py:350
  12.9 19.1 %collective-permute-start.7 = (bf16[128,384]{1,0:T(8,128)(2,1)}, bf16[128,384]{1,0:T(8,128)(2,1)}, u32[]{:S(2)}, u32[]{:S(2)}) collective-permute-start(bf16[128,384]{1,0:T(8,128)(2,1)} %get-tuple-element.48), channel_id=1, source_target_pairs={{0,2},{2,0},{4,6},{6,4},{1,3},{3,1},{5,7},{7,5},{8,10},{10,8},{12,... | collective-permute-start | bytes 294920 | tf_op jit(solution)/shard_map/ppermute | solution.py:350
  14.4 18.9 %collective-permute-start.8 = (bf16[128,384]{1,0:T(8,128)(2,1)}, bf16[128,384]{1,0:T(8,128)(2,1)}, u32[]{:S(2)}, u32[]{:S(2)}) collective-permute-start(bf16[128,384]{1,0:T(8,128)(2,1)} %get-tuple-element.49), channel_id=1, source_target_pairs={{0,4},{2,6},{4,0},{6,2},{1,5},{3,7},{5,1},{7,3},{8,12},{10,14},{12... | collective-permute-start | bytes 294920 | tf_op jit(solution)/shard_map/ppermute | solution.py:350
  28.4 10.7 %collective-permute-start.12 = (f32[256,128]{1,0:T(8,128)S(1)}, f32[256,128]{1,0:T(8,128)S(1)}, u32[]{:S(2)}, u32[]{:S(2)}) collective-permute-start(f32[256,128]{1,0:T(8,128)S(1)} %get-tuple-element.51.a_5_), channel_id=1, source_target_pairs={{0,6},{2,4},{4,2},{6,0},{1,7},{3,5},{5,3},{7,1},{8,14},{10,12},{12... | collective-permute-start | bytes 393224 | tf_op jit(solution)/shard_map/ppermute | solution.py:350
  29.9 9.7 %collective-permute-start.11 = (f32[256,128]{1,0:T(8,128)S(1)}, f32[256,128]{1,0:T(8,128)S(1)}, u32[]{:S(2)}, u32[]{:S(2)}) collective-permute-start(f32[256,128]{1,0:T(8,128)S(1)} %get-tuple-element.51.a_5_), channel_id=1, source_target_pairs={{0,4},{2,6},{4,0},{6,2},{1,5},{3,7},{5,1},{7,3},{8,12},{10,14},{12... | collective-permute-start | bytes 393224 | tf_op jit(solution)/shard_map/ppermute | solution.py:350
  30.7 9.0 %collective-permute-start.10 = (f32[256,128]{1,0:T(8,128)S(1)}, f32[256,128]{1,0:T(8,128)S(1)}, u32[]{:S(2)}, u32[]{:S(2)}) collective-permute-start(f32[256,128]{1,0:T(8,128)S(1)} %get-tuple-element.51.a_5_), channel_id=1, source_target_pairs={{0,2},{2,0},{4,6},{6,4},{1,3},{3,1},{5,7},{7,5},{8,10},{10,8},{12,... | collective-permute-start | bytes 393224 | tf_op jit(solution)/shard_map/ppermute | solution.py:350
  32.0 16.1 %collective-permute-start.33 = (f16[256,512]{1,0:T(8,128)(2,1)S(1)}, f16[256,512]{1,0:T(8,128)(2,1)S(1)}, u32[]{:S(2)}, u32[]{:S(2)}) collective-permute-start(f16[256,512]{1,0:T(8,128)(2,1)S(1)} %fusion), channel_id=1, source_target_pairs={{0,8},{8,0},{16,24},{24,16},{1,9},{9,1},{17,25},{25,17},{2,10},{10... | collective-permute-start | bytes 786440 | tf_op jit(solution)/shard_map/ppermute | solution.py:350
  40.8 35.7 %collective-permute-start.38 = (f16[256,512]{1,0:T(8,128)(2,1)S(1)}, f16[256,512]{1,0:T(8,128)(2,1)S(1)}, u32[]{:S(2)}, u32[]{:S(2)}) collective-permute-start(f16[256,512]{1,0:T(8,128)(2,1)S(1)} %fusion), channel_id=1, source_target_pairs={{0,24},{8,16},{16,8},{24,0},{1,25},{9,17},{17,9},{25,1},{2,26},{10... | collective-permute-start | bytes 786440 | tf_op jit(solution)/shard_map/ppermute | solution.py:350
  43.5 35.6 %collective-permute-start.37 = (f16[256,512]{1,0:T(8,128)(2,1)S(1)}, f16[256,512]{1,0:T(8,128)(2,1)S(1)}, u32[]{:S(2)}, u32[]{:S(2)}) collective-permute-start(f16[256,512]{1,0:T(8,128)(2,1)S(1)} %fusion), channel_id=1, source_target_pairs={{0,16},{8,24},{16,0},{24,8},{1,17},{9,25},{17,1},{25,9},{2,18},{10... | collective-permute-start | bytes 786440 | tf_op jit(solution)/shard_map/ppermute | solution.py:350
  45.1 12.9 %collective-permute-start.17 = (f32[64,384]{1,0:T(8,128)S(1)}, f32[64,384]{1,0:T(8,128)S(1)}, u32[]{:S(2)}, u32[]{:S(2)}) collective-permute-start(f32[64,384]{1,0:T(8,128)S(1)} %get-tuple-element.53), channel_id=1, source_target_pairs={{0,8},{8,0},{16,24},{24,16},{1,9},{9,1},{17,25},{25,17},{2,10},{10... | collective-permute-start | bytes 294920 | tf_op jit(solution)/shard_map/ppermute | solution.py:350
  46.9 26.8 %collective-permute-start.18 = (f32[64,384]{1,0:T(8,128)S(1)}, f32[64,384]{1,0:T(8,128)S(1)}, u32[]{:S(2)}, u32[]{:S(2)}) collective-permute-start(f32[64,384]{1,0:T(8,128)S(1)} %get-tuple-element.54), channel_id=1, source_target_pairs={{0,16},{8,24},{16,0},{24,8},{1,17},{9,25},{17,1},{25,9},{2,18},{10... | collective-permute-start | bytes 294920 | tf_op jit(solution)/shard_map/ppermute | solution.py:350
  48.1 26.8 %collective-permute-start.19 = (f32[64,384]{1,0:T(8,128)S(1)}, f32[64,384]{1,0:T(8,128)S(1)}, u32[]{:S(2)}, u32[]{:S(2)}) collective-permute-start(f32[64,384]{1,0:T(8,128)S(1)} %get-tuple-element.55), channel_id=1, source_target_pairs={{0,24},{8,16},{16,8},{24,0},{1,25},{9,17},{17,9},{25,1},{2,26},{10... | collective-permute-start | bytes 294920 | tf_op jit(solution)/shard_map/ppermute | solution.py:350
  58.0 36.3 %collective-permute-start.36 = (f16[256,512]{1,0:T(8,128)(2,1)S(1)}, f16[256,512]{1,0:T(8,128)(2,1)S(1)}, u32[]{:S(2)}, u32[]{:S(2)}) collective-permute-start(f16[256,512]{1,0:T(8,128)(2,1)S(1)} %multiply_convert_fusion), channel_id=1, source_target_pairs={{0,8},{8,0},{16,24},{24,16},{1,9},{9,1},{17,25},{25,17},{2,10},{10... | collective-permute-start | bytes 786440 | tf_op jit(solution)/shard_map/ppermute | solution.py:350
  73.7 21.2 %collective-permute-start.35 = (f16[256,512]{1,0:T(8,128)(2,1)S(1)}, f16[256,512]{1,0:T(8,128)(2,1)S(1)}, u32[]{:S(2)}, u32[]{:S(2)}) collective-permute-start(f16[256,512]{1,0:T(8,128)(2,1)S(1)} %collective-permute-done.33), channel_id=1, source_target_pairs={{0,4},{2,6},{4,0},{6,2},{1,5},{3,7},{5,1},{7,3},{8,12},{10,14},{12... | collective-permute-start | bytes 786440 | tf_op jit(solution)/shard_map/ppermute | solution.py:350
  74.9 21.4 %collective-permute-start.34 = (f16[256,512]{1,0:T(8,128)(2,1)S(1)}, f16[256,512]{1,0:T(8,128)(2,1)S(1)}, u32[]{:S(2)}, u32[]{:S(2)}) collective-permute-start(f16[256,512]{1,0:T(8,128)(2,1)S(1)} %collective-permute-done.33), channel_id=1, source_target_pairs={{0,2},{2,0},{4,6},{6,4},{1,3},{3,1},{5,7},{7,5},{8,10},{10,8},{12,... | collective-permute-start | bytes 786440 | tf_op jit(solution)/shard_map/ppermute | solution.py:350
  79.0 38.0 %collective-permute-start.6 = (bf16[3072,128]{1,0:T(8,128)(2,1)S(1)}, bf16[3072,128]{1,0:T(8,128)(2,1)S(1)}, u32[]{:S(2)}, u32[]{:S(2)}) collective-permute-start(bf16[3072,128]{1,0:T(8,128)(2,1)S(1)} %get-tuple-element.46.mine), channel_id=1, source_target_pairs={{0,1},{1,0},{2,3},{3,2},{4,5},{5,4},{6,7},{7,6},{8,9},{9,8},{10,11... | collective-permute-start | bytes 2359304 | tf_op jit(solution)/shard_map/ppermute | solution.py:350
  94.3 8.7 %collective-permute-start.39 = (f16[256,512]{1,0:T(8,128)(2,1)S(1)}, f16[256,512]{1,0:T(8,128)(2,1)S(1)}, u32[]{:S(2)}, u32[]{:S(2)}) collective-permute-start(f16[256,512]{1,0:T(8,128)(2,1)S(1)} %collective-permute-done.37), channel_id=1, source_target_pairs={{0,2},{2,0},{4,6},{6,4},{1,3},{3,1},{5,7},{7,5},{8,10},{10,8},{12,... | collective-permute-start | bytes 786440 | tf_op jit(solution)/shard_map/ppermute | solution.py:350
  97.4 9.4 %collective-permute-start.40 = (f16[256,512]{1,0:T(8,128)(2,1)S(1)}, f16[256,512]{1,0:T(8,128)(2,1)S(1)}, u32[]{:S(2)}, u32[]{:S(2)}) collective-permute-start(f16[256,512]{1,0:T(8,128)(2,1)S(1)} %collective-permute-done.38), channel_id=1, source_target_pairs={{0,2},{2,0},{4,6},{6,4},{1,3},{3,1},{5,7},{7,5},{8,10},{10,8},{12,... | collective-permute-start | bytes 786440 | tf_op jit(solution)/shard_map/ppermute | solution.py:350
  103.0 11.1 %collective-permute-start.32 = (f32[64,384]{1,0:T(8,128)S(1)}, f32[64,384]{1,0:T(8,128)S(1)}, u32[]{:S(2)}, u32[]{:S(2)}) collective-permute-start(f32[64,384]{1,0:T(8,128)S(1)} %get-tuple-element.59.a_10_), channel_id=1, source_target_pairs={{0,6},{2,4},{4,2},{6,0},{1,7},{3,5},{5,3},{7,1},{8,14},{10,12},{12... | collective-permute-start | bytes 294920 | tf_op jit(solution)/shard_map/ppermute | solution.py:350
  114.0 9.5 %collective-permute-start.24 = (bf16[256,384]{1,0:T(8,128)(2,1)S(1)}, bf16[256,384]{1,0:T(8,128)(2,1)S(1)}, u32[]{:S(2)}, u32[]{:S(2)}) collective-permute-start(bf16[256,384]{1,0:T(8,128)(2,1)S(1)} %get-tuple-element.57.a_2_), channel_id=1, source_target_pairs={{0,4},{2,6},{4,0},{6,2},{1,5},{3,7},{5,1},{7,3},{8,12},{10,14},{12... | collective-permute-start | bytes 589832 | tf_op jit(solution)/shard_map/ppermute | solution.py:350
  115.0 9.9 %collective-permute-start.23 = (bf16[256,384]{1,0:T(8,128)(2,1)S(1)}, bf16[256,384]{1,0:T(8,128)(2,1)S(1)}, u32[]{:S(2)}, u32[]{:S(2)}) collective-permute-start(bf16[256,384]{1,0:T(8,128)(2,1)S(1)} %get-tuple-element.57.a_2_), channel_id=1, source_target_pairs={{0,2},{2,0},{4,6},{6,4},{1,3},{3,1},{5,7},{7,5},{8,10},{10,8},{12,... | collective-permute-start | bytes 589832 | tf_op jit(solution)/shard_map/ppermute | solution.py:350
  115.9 13.8 %collective-permute-start.44 = (f16[256,512]{1,0:T(8,128)(2,1)S(1)}, f16[256,512]{1,0:T(8,128)(2,1)S(1)}, u32[]{:S(2)}, u32[]{:S(2)}) collective-permute-start(f16[256,512]{1,0:T(8,128)(2,1)S(1)} %pad_maximum_fusion.1), channel_id=1, source_target_pairs={{0,2},{2,0},{4,6},{6,4},{1,3},{3,1},{5,7},{7,5},{8,10},{10,8},{12,... | collective-permute-start | bytes 786440 | tf_op jit(solution)/shard_map/ppermute | solution.py:350
  117.0 12.8 %collective-permute-start.43 = (f16[256,512]{1,0:T(8,128)(2,1)S(1)}, f16[256,512]{1,0:T(8,128)(2,1)S(1)}, u32[]{:S(2)}, u32[]{:S(2)}) collective-permute-start(f16[256,512]{1,0:T(8,128)(2,1)S(1)} %pad_maximum_fusion), channel_id=1, source_target_pairs={{0,4},{2,6},{4,0},{6,2},{1,5},{3,7},{5,1},{7,3},{8,12},{10,14},{12... | collective-permute-start | bytes 786440 | tf_op jit(solution)/shard_map/ppermute | solution.py:350
  (41 other events, 415.6 us)
where the time goes:
time: 132 us
  waiting for transfers between devices  57 us (43%)
  starting transfers between devices  50.1 us (38%)
  Pallas kernels  14.3 us (11%)
  local copies, waits for them, and re-layouts  7.89 us (6%)
    ppermute x45, waiting for transfers between devices, swap(): return lax.ppermute(x, axis, [(i, i ^ m) for i in range(n)])  57 us
    ppermute x45, starting transfers between devices, swap(): return lax.ppermute(x, axis, [(i, i ^ m) for i in range(n)])  50.1 us
    pallas_call x8, Pallas kernels, call(): pl.pallas_call(kernel, out_shape=outs, in_specs=[SMEM] + [source] * (len(...  7.79 us
    unnamed x42, local copies, waits for them, and re-layouts  6.09 us
    pallas_call x1, Pallas kernels, local_short(): pl.pallas_call(lambda *a: step_kernel(nf, nr, block_q, count, *a), out_sh...  4.87 us
  transfers between devices with their start and end apart: 45, of which 16 were waited for; matrix products, arithmetic and copies ran while one was open for 2% of the time, Pallas kernels for 9%

commit v1 on v0

--- a/solution.py
+++ b/solution.py
@@ -70,17 +70,16 @@
         copy.wait()
 
 
-def share_kernel(nr, place, proj_q, proj_o, out, sems):
+def share_kernel(nr, place, proj_q, proj_o, share, both, sems):
     r, t = place[1], place[2]
-    part_q, part_o, half = proj_q.shape[0] // nr, proj_o.shape[0] // nr, out.shape[1]
+    part_q, part_o, half = proj_q.shape[0] // nr, proj_o.shape[0] // nr, share.shape[1]
+    part = part_q + part_o
     mine = pl.ds(pl.multiple_of(t * half, half), half)
-    fetch(
-        [
-            (proj_q.at[pl.ds(pl.multiple_of(r * part_q, part_q), part_q), mine], out.at[0:part_q, :]),
-            (proj_o.at[pl.ds(pl.multiple_of(r * part_o, part_o), part_o), mine], out.at[part_q : part_q + part_o, :]),
-        ],
-        sems,
-    )
+    pairs = []
+    for at, out, base in ((r, share, 0), (r, both, 0), (r ^ (nr - 1), both, part)):
+        pairs.append((proj_q.at[pl.ds(pl.multiple_of(at * part_q, part_q), part_q), mine], out.at[base : base + part_q, :]))
+        pairs.append((proj_o.at[pl.ds(pl.multiple_of(at * part_o, part_o), part_o), mine], out.at[base + part_q : base + part, :]))
+    fetch(pairs, sems)
 
 
 def cot_kernel(nr, place, cot_q, cot_o, *rest):
@@ -108,7 +107,7 @@
 
 
 def reduce_kernel(nf, nr, place, inputs, attended, proj_q, proj_o, own, *rest):
-    near, (table, red) = rest[:-2], rest[-2:]
+    near, (both, table, red) = rest[:-3], rest[-3:]
     f, r, t = place[0], place[1], place[2]
     half = table.shape[1]
     rows_q, rows_o = proj_q.shape[0], proj_o.shape[0]
@@ -118,10 +117,12 @@
     mine = pl.ds(pl.multiple_of(t * half, half), half)
     table[pl.ds(pl.multiple_of(f * rows_q, rows_q), rows_q), :] = proj_q[:, mine]
     table[pl.ds(pl.multiple_of(cut + f * rows_o, rows_o), rows_o), :] = proj_o[:, mine]
-    for mr, ref in enumerate((own,) + near):
+    for mr, whole in enumerate((own,) + near):
         for mz in range(1, nf):
             at = (f ^ mz) * nr + (r ^ mr)
-            base = (mz - 1) * part
+            ref, base = whole, (mz - 1) * part
+            if mr == nr - 1:
+                ref, base = (both, part) if mz == 1 else (whole, base - part)
             table[pl.ds(pl.multiple_of(at * part_q, part_q), part_q), :] = ref[base : base + part_q, :]
             table[pl.ds(pl.multiple_of(cut + at * part_o, part_o), part_o), :] = ref[base + part_q : base + part, :]
     red_q = jnp.dot(inputs[...], table[0:cut, :], preferred_element_type=f32)
@@ -349,16 +350,17 @@
     def swap(x, axis, m, n):
         return lax.ppermute(x, axis, [(i, i ^ m) for i in range(n)])
 
-    fs_order = list(range(nf - 1, 0, -1))
-    rep_order = list(range(nr - 1, 0, -1))
+    def batch(make, axis, n):
+        got = {}
+        for m in range(n - 1, 0, -1):
+            got[m] = swap(make(m), axis, m, n)
+        return [got[m] for m in range(1, n)]
 
     def over_fs(make):
-        got = {m: swap(make(m), "fs", m, nf) for m in fs_order}
-        return [got[m] for m in range(1, nf)]
+        return batch(make, "fs", nf)
 
     def over_rep(make):
-        got = {m: swap(make(m), "rep", m, nr) for m in rep_order}
-        return [got[m] for m in range(1, nr)]
+        return batch(make, "rep", nr)
 
     def over_tp(x):
         return swap(x, "tp", 1, 2)
@@ -373,14 +375,15 @@
     block = block_q + block_o
     rows = rank // nf
 
-    share = call(
+    part = part_q + part_o
+    share, both = call(
         lambda *a: share_kernel(nr, *a),
-        shape((part_q + part_o, half), bf16),
+        [shape((part, half), bf16), shape((2 * part, half), bf16)],
         (place, proj_query, proj_output),
-        scratch=[pltpu.SemaphoreType.DMA((2,))],
+        scratch=[pltpu.SemaphoreType.DMA((6,))],
         source=ANY,
     )
-    far = over_fs(lambda m: share)
+    both, *far = over_fs(lambda m: both if m == 1 else share)
 
     def encode(at, old_q, old_o):
         parts = [lax.dynamic_slice(old_q, (at * part_q, 0), (part_q, cols_q))]
@@ -389,7 +392,8 @@
         return (jnp.concatenate(parts, axis=0) * code_scale).astype(jnp.float16)
 
     code = encode(r, weight_query, weight_output)
-    code_far = {m: swap(code, "fs", m, nf) for m in range(1, nf)}
+    code_far = {1: swap(code, "fs", 1, nf)}
+    code_far |= {m: swap(code, "fs", m, nf) for m in range(2, nf)}
 
     cots = call(
         lambda *a: cot_kernel(nr, *a),
@@ -410,13 +414,14 @@
     corner = (corner * code_scale).astype(jnp.float16)
     corners = {1: swap(corner, "fs", 1, nf)}
 
-    own = jnp.concatenate(far, axis=0)
-    near = over_rep(lambda m: own)
+    own = jnp.concatenate([both[:part], *far], axis=0)
+    farther = jnp.concatenate(far, axis=0)
+    near = over_rep(lambda m: own if m < nr - 1 else farther)
 
     table, red = call(
         lambda *a: reduce_kernel(nf, nr, *a),
         [shape(((rows_q + rows_o) * nf, half), bf16), shape((2 * half, tokens))],
-        (place, inputs, attended, proj_query, proj_output, own, *near),
+        (place, inputs, attended, proj_query, proj_output, own, *near, both),
     )
     mine = [red] + over_rep(lambda m: red)
     other = [over_tp(x) for x in mine]

time: 132 us -> 127 us (0.962)
  local copies, waits for them, and re-layouts: 7.89 us -> 4.92 us
  Pallas kernels: 14.3 us -> 12.8 us
    unnamed x42 -> x28, local copies, waits for them, and re-layouts: 6.09 us -> 3.83 us
    pallas_call x8, Pallas kernels: 7.79 us -> 6.35 us  [call(): pl.pallas_call(kernel, out_shape=outs, in_specs=[SMEM] + [source] * (len(...]
  transfers between devices with their start and end apart: 45 -> 45, of which waited for: 16 -> 15; matrix products, arithmetic and copies ran while one was open for 2% -> 2% of each run, Pallas kernels for 9% -> 8%
where the time goes in v1:
time: 127 us
  waiting for transfers between devices  56.1 us (44%)
  starting transfers between devices  51.2 us (40%)
  Pallas kernels  12.8 us (10%)
  local copies, waits for them, and re-layouts  4.92 us (4%)
    ppermute x45, waiting for transfers between devices, swap(): return lax.ppermute(x, axis, [(i, i ^ m) for i in range(n)])  56.1 us
    ppermute x45, starting transfers between devices, swap(): return lax.ppermute(x, axis, [(i, i ^ m) for i in range(n)])  51.2 us
    pallas_call x8, Pallas kernels, call(): pl.pallas_call(kernel, out_shape=outs, in_specs=[SMEM] + [source] * (len(...  6.35 us
    pallas_call x1, Pallas kernels, local_short(): pl.pallas_call(lambda *a: step_kernel(nf, nr, block_q, count, *a), out_sh...  4.83 us
    unnamed x28, local copies, waits for them, and re-layouts  3.83 us
  transfers between devices with their start and end apart: 45, of which 15 were waited for; matrix products, arithmetic and copies ran while one was open for 2% of the time, Pallas kernels for 8%

profile of v1, /device:TPU:0, one launch (start us, length us, event | category | flops | bytes accessed | tf_op | source)
XLA Modules:
  0.0 127.3 jit_solution(12420322231567530693)
XLA Ops:
  3.3 5.1 %collective-permute-start.2 = (bf16[192,128]{1,0:T(8,128)(2,1)S(1)}, bf16[192,128]{1,0:T(8,128)(2,1)S(1)}, u32[]{:S(2)}, u32[]{:S(2)}) collective-permute-start(bf16[192,128]{1,0:T(8,128)(2,1)S(1)} %get-tuple-element.49), channel_id=1, source_target_pairs={{0,24},{8,16},{16,8},{24,0},{1,25},{9,17},{17,9},{25,1},{2,26},{10... | collective-permute-start | bytes 147464 | tf_op jit(solution)/shard_map/ppermute | solution.py:351
  11.7 1.7 %collective-permute-start.7 = (bf16[128,384]{1,0:T(8,128)(2,1)S(1)}, bf16[128,384]{1,0:T(8,128)(2,1)S(1)}, u32[]{:S(2)}, u32[]{:S(2)}) collective-permute-start(bf16[128,384]{1,0:T(8,128)(2,1)S(1)} %get-tuple-element.52), channel_id=1, source_target_pairs={{0,2},{2,0},{4,6},{6,4},{1,3},{3,1},{5,7},{7,5},{8,10},{10,8},{12,... | collective-permute-start | bytes 294920 | tf_op jit(solution)/shard_map/ppermute | solution.py:351
  17.1 2.5 %collective-permute-start.5 = (bf16[384,128]{1,0:T(8,128)(2,1)S(1)}, bf16[384,128]{1,0:T(8,128)(2,1)S(1)}, u32[]{:S(2)}, u32[]{:S(2)}) collective-permute-start(bf16[384,128]{1,0:T(8,128)(2,1)S(1)} %pad_maximum_fusion.3), channel_id=1, source_target_pairs={{0,6},{2,4},{4,2},{6,0},{1,7},{3,5},{5,3},{7,1},{8,14},{10,12},{12... | collective-permute-start | bytes 294920 | tf_op jit(solution)/shard_map/ppermute | solution.py:351
  19.6 4.1 %collective-permute-done.5.a_8_ = bf16[384,128]{1,0:T(8,128)(2,1)S(1)} collective-permute-done((bf16[384,128]{1,0:T(8,128)(2,1)S(1)}, bf16[384,128]{1,0:T(8,128)(2,1)S(1)}, u32[]{:S(2)}, u32[]{:S(2)}) %collective-permute-start.5) | collective-permute-done | bytes 98336 | tf_op jit(solution)/shard_map/ppermute | solution.py:351
  31.1 4.2 %collective-permute-done.9.a_4_ = bf16[128,384]{1,0:T(8,128)(2,1)S(1)} collective-permute-done((bf16[128,384]{1,0:T(8,128)(2,1)S(1)}, bf16[128,384]{1,0:T(8,128)(2,1)S(1)}, u32[]{:S(2)}, u32[]{:S(2)}) %collective-permute-start.9) | collective-permute-done | bytes 98336 | tf_op jit(solution)/shard_map/ppermute | solution.py:351
  37.1 2.4 %collective-permute-start.38 = (f16[256,512]{1,0:T(8,128)(2,1)S(1)}, f16[256,512]{1,0:T(8,128)(2,1)S(1)}, u32[]{:S(2)}, u32[]{:S(2)}) collective-permute-start(f16[256,512]{1,0:T(8,128)(2,1)S(1)} %fusion), channel_id=1, source_target_pairs={{0,24},{8,16},{16,8},{24,0},{1,25},{9,17},{17,9},{25,1},{2,26},{10... | collective-permute-start | bytes 786440 | tf_op jit(solution)/shard_map/ppermute | solution.py:351
  41.2 1.6 %collective-permute-start.17 = (f32[64,384]{1,0:T(8,128)S(1)}, f32[64,384]{1,0:T(8,128)S(1)}, u32[]{:S(2)}, u32[]{:S(2)}) collective-permute-start(f32[64,384]{1,0:T(8,128)S(1)} %get-tuple-element.57), channel_id=1, source_target_pairs={{0,8},{8,0},{16,24},{24,16},{1,9},{9,1},{17,25},{25,17},{2,10},{10... | collective-permute-start | bytes 294920 | tf_op jit(solution)/shard_map/ppermute | solution.py:351
  42.8 1.9 %collective-permute-start.18 = (f32[64,384]{1,0:T(8,128)S(1)}, f32[64,384]{1,0:T(8,128)S(1)}, u32[]{:S(2)}, u32[]{:S(2)}) collective-permute-start(f32[64,384]{1,0:T(8,128)S(1)} %get-tuple-element.58), channel_id=1, source_target_pairs={{0,16},{8,24},{16,0},{24,8},{1,17},{9,25},{17,1},{25,9},{2,18},{10... | collective-permute-start | bytes 294920 | tf_op jit(solution)/shard_map/ppermute | solution.py:351
  45.7 8.3 %collective-permute-done.17.a_2_ = f32[64,384]{1,0:T(8,128)S(1)} collective-permute-done((f32[64,384]{1,0:T(8,128)S(1)}, f32[64,384]{1,0:T(8,128)S(1)}, u32[]{:S(2)}, u32[]{:S(2)}) %collective-permute-start.17) | collective-permute-done | bytes 98336 | tf_op jit(solution)/shard_map/ppermute | solution.py:351
  54.0 2.5 %collective-permute-start.36 = (f16[256,512]{1,0:T(8,128)(2,1)S(1)}, f16[256,512]{1,0:T(8,128)(2,1)S(1)}, u32[]{:S(2)}, u32[]{:S(2)}) collective-permute-start(f16[256,512]{1,0:T(8,128)(2,1)S(1)} %multiply_convert_fusion), channel_id=1, source_target_pairs={{0,8},{8,0},{16,24},{24,16},{1,9},{9,1},{17,25},{25,17},{2,10},{10... | collective-permute-start | bytes 786440 | tf_op jit(solution)/shard_map/ppermute | solution.py:351
  56.5 13.8 %collective-permute-done.18.a_3_ = f32[64,384]{1,0:T(8,128)S(1)} collective-permute-done((f32[64,384]{1,0:T(8,128)S(1)}, f32[64,384]{1,0:T(8,128)S(1)}, u32[]{:S(2)}, u32[]{:S(2)}) %collective-permute-start.18) | collective-permute-done | bytes 98336 | tf_op jit(solution)/shard_map/ppermute | solution.py:351
  73.1 2.6 %collective-permute-start.22 = (bf16[80,384]{1,0:T(8,128)(2,1)S(1)}, bf16[80,384]{1,0:T(8,128)(2,1)S(1)}, u32[]{:S(2)}, u32[]{:S(2)}) collective-permute-start(bf16[80,384]{1,0:T(8,128)(2,1)S(1)} %get-tuple-element.60.a_1_), channel_id=1, source_target_pairs={{0,24},{8,16},{16,8},{24,0},{1,25},{9,17},{17,9},{25,1},{2,26},{10... | collective-permute-start | bytes 184328 | tf_op jit(solution)/shard_map/ppermute | solution.py:351
  75.7 3.5 %collective-permute-done.22.a_4_ = bf16[80,384]{1,0:T(8,128)(2,1)S(1)} collective-permute-done((bf16[80,384]{1,0:T(8,128)(2,1)S(1)}, bf16[80,384]{1,0:T(8,128)(2,1)S(1)}, u32[]{:S(2)}, u32[]{:S(2)}) %collective-permute-start.22) | collective-permute-done | bytes 61472 | tf_op jit(solution)/shard_map/ppermute | solution.py:351
  79.2 5.5 %collective-permute-done.21.a_3_ = bf16[80,384]{1,0:T(8,128)(2,1)S(1)} collective-permute-done((bf16[80,384]{1,0:T(8,128)(2,1)S(1)}, bf16[80,384]{1,0:T(8,128)(2,1)S(1)}, u32[]{:S(2)}, u32[]{:S(2)}) %collective-permute-start.21) | collective-permute-done | bytes 61472 | tf_op jit(solution)/shard_map/ppermute | solution.py:351
  84.7 4.2 %collective-permute-done.20.a_2_ = bf16[80,384]{1,0:T(8,128)(2,1)S(1)} collective-permute-done((bf16[80,384]{1,0:T(8,128)(2,1)S(1)}, bf16[80,384]{1,0:T(8,128)(2,1)S(1)}, u32[]{:S(2)}, u32[]{:S(2)}) %collective-permute-start.20) | collective-permute-done | bytes 61472 | tf_op jit(solution)/shard_map/ppermute | solution.py:351
  90.0 1.6 %collective-permute-start.39 = (f16[256,512]{1,0:T(8,128)(2,1)S(1)}, f16[256,512]{1,0:T(8,128)(2,1)S(1)}, u32[]{:S(2)}, u32[]{:S(2)}) collective-permute-start(f16[256,512]{1,0:T(8,128)(2,1)S(1)} %collective-permute-done.37), channel_id=1, source_target_pairs={{0,2},{2,0},{4,6},{6,4},{1,3},{3,1},{5,7},{7,5},{8,10},{10,8},{12,... | collective-permute-start | bytes 786440 | tf_op jit(solution)/shard_map/ppermute | solution.py:351
  98.9 1.6 %collective-permute-start.32 = (f32[64,384]{1,0:T(8,128)S(1)}, f32[64,384]{1,0:T(8,128)S(1)}, u32[]{:S(2)}, u32[]{:S(2)}) collective-permute-start(f32[64,384]{1,0:T(8,128)S(1)} %get-tuple-element.63.a_10_), channel_id=1, source_target_pairs={{0,6},{2,4},{4,2},{6,0},{1,7},{3,5},{5,3},{7,1},{8,14},{10,12},{12... | collective-permute-start | bytes 294920 | tf_op jit(solution)/shard_map/ppermute | solution.py:351
  100.6 2.0 %collective-permute-done.40 = f16[256,512]{1,0:T(8,128)(2,1)S(1)} collective-permute-done((f16[256,512]{1,0:T(8,128)(2,1)S(1)}, f16[256,512]{1,0:T(8,128)(2,1)S(1)}, u32[]{:S(2)}, u32[]{:S(2)}) %collective-permute-start.40) | collective-permute-done | bytes 262176 | tf_op jit(solution)/shard_map/ppermute | solution.py:351
  104.6 1.6 %collective-permute-start.27 = (f32[8,128]{1,0:T(8,128)S(1)}, f32[8,128]{1,0:T(8,128)S(1)}, u32[]{:S(2)}, u32[]{:S(2)}) collective-permute-start(f32[8,128]{1,0:T(8,128)S(1)} %add.10.a_6_), channel_id=1, source_target_pairs={{0,2},{2,0},{4,6},{6,4},{1,3},{3,1},{5,7},{7,5},{8,10},{10,8},{12,... | collective-permute-start | bytes 12296 | tf_op jit(solution)/shard_map/ppermute | solution.py:351
  106.2 2.6 %collective-permute-done.27.a_7_ = f32[8,128]{1,0:T(8,128)S(1)} collective-permute-done((f32[8,128]{1,0:T(8,128)S(1)}, f32[8,128]{1,0:T(8,128)S(1)}, u32[]{:S(2)}, u32[]{:S(2)}) %collective-permute-start.27) | collective-permute-done | bytes 4128 | tf_op jit(solution)/shard_map/ppermute | solution.py:351
  115.8 1.7 %collective-permute-done.25.a_5_ = bf16[256,384]{1,0:T(8,128)(2,1)S(1)} collective-permute-done((bf16[256,384]{1,0:T(8,128)(2,1)S(1)}, bf16[256,384]{1,0:T(8,128)(2,1)S(1)}, u32[]{:S(2)}, u32[]{:S(2)}) %collective-permute-start.25) | collective-permute-done | bytes 196640 | tf_op jit(solution)/shard_map/ppermute | solution.py:351
  117.5 2.4 %collective-permute-done.24.a_4_ = bf16[256,384]{1,0:T(8,128)(2,1)S(1)} collective-permute-done((bf16[256,384]{1,0:T(8,128)(2,1)S(1)}, bf16[256,384]{1,0:T(8,128)(2,1)S(1)}, u32[]{:S(2)}, u32[]{:S(2)}) %collective-permute-start.24) | collective-permute-done | bytes 196640 | tf_op jit(solution)/shard_map/ppermute | solution.py:351
  120.6 4.8 %step.1 = (bf16[2048,512]{1,0:T(8,128)(2,1)}, bf16[1024,1024]{1,0:T(8,128)(2,1)}, f32[512,512]{1,0:T(8,128)}, f32[256,1024]{1,0:T(8,128)}, f32[512,512]{1,0:T(8,...) custom-call(s32[3]{0:T(128)S(1)} %pad_add_fusion.a_0_.place, ...), custom_call_target="tpu_custom_call" | custom-call | tf_op jit(solution)/shard_map/step/pallas_call | solution.py:470
  125.6 1.6 %corner.1 = (bf16[2048,512]{1,0:T(8,128)(2,1)}, bf16[1024,1024]{1,0:T(8,128)(2,1)}) custom-call(s32[3]{0:T(128)S(1)} %pad_add_fusion.a_0_.place, bf16[3072,256]{1,0:T(8,128)(2,1)S(1)} %shard_map.197.a_1_, bf16[256,1536]{1,0:T(8,128)(2,1)S(1)} %get-tuple-element.78.a_2_, ...), custom_call_target="tpu_custom_call", output_to_operand_aliasing={{0}: (6, {}), {1}: (7, {})} | custom-call | tf_op jit(solution)/shard_map/corner/pallas_call | solution.py:503
  (124 shorter events, 42.4 us)
Async XLA Ops:
  3.3 12.6 %collective-permute-start.2 = (bf16[192,128]{1,0:T(8,128)(2,1)S(1)}, bf16[192,128]{1,0:T(8,128)(2,1)S(1)}, u32[]{:S(2)}, u32[]{:S(2)}) collective-permute-start(bf16[192,128]{1,0:T(8,128)(2,1)S(1)} %get-tuple-element.49), channel_id=1, source_target_pairs={{0,24},{8,16},{16,8},{24,0},{1,25},{9,17},{17,9},{25,1},{2,26},{10... | collective-permute-start | bytes 147464 | tf_op jit(solution)/shard_map/ppermute | solution.py:351
  11.7 16.7 %collective-permute-start.7 = (bf16[128,384]{1,0:T(8,128)(2,1)S(1)}, bf16[128,384]{1,0:T(8,128)(2,1)S(1)}, u32[]{:S(2)}, u32[]{:S(2)}) collective-permute-start(bf16[128,384]{1,0:T(8,128)(2,1)S(1)} %get-tuple-element.52), channel_id=1, source_target_pairs={{0,2},{2,0},{4,6},{6,4},{1,3},{3,1},{5,7},{7,5},{8,10},{10,8},{12,... | collective-permute-start | bytes 294920 | tf_op jit(solution)/shard_map/ppermute | solution.py:351
  13.4 16.4 %collective-permute-start.8 = (bf16[128,384]{1,0:T(8,128)(2,1)S(1)}, bf16[128,384]{1,0:T(8,128)(2,1)S(1)}, u32[]{:S(2)}, u32[]{:S(2)}) collective-permute-start(bf16[128,384]{1,0:T(8,128)(2,1)S(1)} %get-tuple-element.53), channel_id=1, source_target_pairs={{0,4},{2,6},{4,0},{6,2},{1,5},{3,7},{5,1},{7,3},{8,12},{10,14},{12... | collective-permute-start | bytes 294920 | tf_op jit(solution)/shard_map/ppermute | solution.py:351
  24.8 10.6 %collective-permute-start.12 = (f32[256,128]{1,0:T(8,128)S(1)}, f32[256,128]{1,0:T(8,128)S(1)}, u32[]{:S(2)}, u32[]{:S(2)}) collective-permute-start(f32[256,128]{1,0:T(8,128)S(1)} %get-tuple-element.55.a_5_), channel_id=1, source_target_pairs={{0,6},{2,4},{4,2},{6,0},{1,7},{3,5},{5,3},{7,1},{8,14},{10,12},{12... | collective-permute-start | bytes 393224 | tf_op jit(solution)/shard_map/ppermute | solution.py:351
  26.3 9.6 %collective-permute-start.11 = (f32[256,128]{1,0:T(8,128)S(1)}, f32[256,128]{1,0:T(8,128)S(1)}, u32[]{:S(2)}, u32[]{:S(2)}) collective-permute-start(f32[256,128]{1,0:T(8,128)S(1)} %get-tuple-element.55.a_5_), channel_id=1, source_target_pairs={{0,4},{2,6},{4,0},{6,2},{1,5},{3,7},{5,1},{7,3},{8,12},{10,14},{12... | collective-permute-start | bytes 393224 | tf_op jit(solution)/shard_map/ppermute | solution.py:351
  26.9 9.0 %collective-permute-start.10 = (f32[256,128]{1,0:T(8,128)S(1)}, f32[256,128]{1,0:T(8,128)S(1)}, u32[]{:S(2)}, u32[]{:S(2)}) collective-permute-start(f32[256,128]{1,0:T(8,128)S(1)} %get-tuple-element.55.a_5_), channel_id=1, source_target_pairs={{0,2},{2,0},{4,6},{6,4},{1,3},{3,1},{5,7},{7,5},{8,10},{10,8},{12,... | collective-permute-start | bytes 393224 | tf_op jit(solution)/shard_map/ppermute | solution.py:351
  28.4 16.3 %collective-permute-start.33 = (f16[256,512]{1,0:T(8,128)(2,1)S(1)}, f16[256,512]{1,0:T(8,128)(2,1)S(1)}, u32[]{:S(2)}, u32[]{:S(2)}) collective-permute-start(f16[256,512]{1,0:T(8,128)(2,1)S(1)} %fusion), channel_id=1, source_target_pairs={{0,8},{8,0},{16,24},{24,16},{1,9},{9,1},{17,25},{25,17},{2,10},{10... | collective-permute-start | bytes 786440 | tf_op jit(solution)/shard_map/ppermute | solution.py:351
  37.1 36.0 %collective-permute-start.38 = (f16[256,512]{1,0:T(8,128)(2,1)S(1)}, f16[256,512]{1,0:T(8,128)(2,1)S(1)}, u32[]{:S(2)}, u32[]{:S(2)}) collective-permute-start(f16[256,512]{1,0:T(8,128)(2,1)S(1)} %fusion), channel_id=1, source_target_pairs={{0,24},{8,16},{16,8},{24,0},{1,25},{9,17},{17,9},{25,1},{2,26},{10... | collective-permute-start | bytes 786440 | tf_op jit(solution)/shard_map/ppermute | solution.py:351
  39.5 36.2 %collective-permute-start.37 = (f16[256,512]{1,0:T(8,128)(2,1)S(1)}, f16[256,512]{1,0:T(8,128)(2,1)S(1)}, u32[]{:S(2)}, u32[]{:S(2)}) collective-permute-start(f16[256,512]{1,0:T(8,128)(2,1)S(1)} %fusion), channel_id=1, source_target_pairs={{0,16},{8,24},{16,0},{24,8},{1,17},{9,25},{17,1},{25,9},{2,18},{10... | collective-permute-start | bytes 786440 | tf_op jit(solution)/shard_map/ppermute | solution.py:351
  41.2 12.8 %collective-permute-start.17 = (f32[64,384]{1,0:T(8,128)S(1)}, f32[64,384]{1,0:T(8,128)S(1)}, u32[]{:S(2)}, u32[]{:S(2)}) collective-permute-start(f32[64,384]{1,0:T(8,128)S(1)} %get-tuple-element.57), channel_id=1, source_target_pairs={{0,8},{8,0},{16,24},{24,16},{1,9},{9,1},{17,25},{25,17},{2,10},{10... | collective-permute-start | bytes 294920 | tf_op jit(solution)/shard_map/ppermute | solution.py:351
  42.8 27.5 %collective-permute-start.18 = (f32[64,384]{1,0:T(8,128)S(1)}, f32[64,384]{1,0:T(8,128)S(1)}, u32[]{:S(2)}, u32[]{:S(2)}) collective-permute-start(f32[64,384]{1,0:T(8,128)S(1)} %get-tuple-element.58), channel_id=1, source_target_pairs={{0,16},{8,24},{16,0},{24,8},{1,17},{9,25},{17,1},{25,9},{2,18},{10... | collective-permute-start | bytes 294920 | tf_op jit(solution)/shard_map/ppermute | solution.py:351
  44.7 26.2 %collective-permute-start.19 = (f32[64,384]{1,0:T(8,128)S(1)}, f32[64,384]{1,0:T(8,128)S(1)}, u32[]{:S(2)}, u32[]{:S(2)}) collective-permute-start(f32[64,384]{1,0:T(8,128)S(1)} %get-tuple-element.59), channel_id=1, source_target_pairs={{0,24},{8,16},{16,8},{24,0},{1,25},{9,17},{17,9},{25,1},{2,26},{10... | collective-permute-start | bytes 294920 | tf_op jit(solution)/shard_map/ppermute | solution.py:351
  54.0 36.0 %collective-permute-start.36 = (f16[256,512]{1,0:T(8,128)(2,1)S(1)}, f16[256,512]{1,0:T(8,128)(2,1)S(1)}, u32[]{:S(2)}, u32[]{:S(2)}) collective-permute-start(f16[256,512]{1,0:T(8,128)(2,1)S(1)} %multiply_convert_fusion), channel_id=1, source_target_pairs={{0,8},{8,0},{16,24},{24,16},{1,9},{9,1},{17,25},{25,17},{2,10},{10... | collective-permute-start | bytes 786440 | tf_op jit(solution)/shard_map/ppermute | solution.py:351
  70.3 21.3 %collective-permute-start.35 = (f16[256,512]{1,0:T(8,128)(2,1)S(1)}, f16[256,512]{1,0:T(8,128)(2,1)S(1)}, u32[]{:S(2)}, u32[]{:S(2)}) collective-permute-start(f16[256,512]{1,0:T(8,128)(2,1)S(1)} %collective-permute-done.33), channel_id=1, source_target_pairs={{0,4},{2,6},{4,0},{6,2},{1,5},{3,7},{5,1},{7,3},{8,12},{10,14},{12... | collective-permute-start | bytes 786440 | tf_op jit(solution)/shard_map/ppermute | solution.py:351
  70.8 21.2 %collective-permute-start.34 = (f16[256,512]{1,0:T(8,128)(2,1)S(1)}, f16[256,512]{1,0:T(8,128)(2,1)S(1)}, u32[]{:S(2)}, u32[]{:S(2)}) collective-permute-start(f16[256,512]{1,0:T(8,128)(2,1)S(1)} %collective-permute-done.33), channel_id=1, source_target_pairs={{0,2},{2,0},{4,6},{6,4},{1,3},{3,1},{5,7},{7,5},{8,10},{10,8},{12,... | collective-permute-start | bytes 786440 | tf_op jit(solution)/shard_map/ppermute | solution.py:351
  75.7 37.6 %collective-permute-start.6 = (bf16[3072,128]{1,0:T(8,128)(2,1)S(1)}, bf16[3072,128]{1,0:T(8,128)(2,1)S(1)}, u32[]{:S(2)}, u32[]{:S(2)}) collective-permute-start(bf16[3072,128]{1,0:T(8,128)(2,1)S(1)} %get-tuple-element.50.mine), channel_id=1, source_target_pairs={{0,1},{1,0},{2,3},{3,2},{4,5},{5,4},{6,7},{7,6},{8,9},{9,8},{10,11... | collective-permute-start | bytes 2359304 | tf_op jit(solution)/shard_map/ppermute | solution.py:351
  90.0 8.9 %collective-permute-start.39 = (f16[256,512]{1,0:T(8,128)(2,1)S(1)}, f16[256,512]{1,0:T(8,128)(2,1)S(1)}, u32[]{:S(2)}, u32[]{:S(2)}) collective-permute-start(f16[256,512]{1,0:T(8,128)(2,1)S(1)} %collective-permute-done.37), channel_id=1, source_target_pairs={{0,2},{2,0},{4,6},{6,4},{1,3},{3,1},{5,7},{7,5},{8,10},{10,8},{12,... | collective-permute-start | bytes 786440 | tf_op jit(solution)/shard_map/ppermute | solution.py:351
  93.2 9.3 %collective-permute-start.40 = (f16[256,512]{1,0:T(8,128)(2,1)S(1)}, f16[256,512]{1,0:T(8,128)(2,1)S(1)}, u32[]{:S(2)}, u32[]{:S(2)}) collective-permute-start(f16[256,512]{1,0:T(8,128)(2,1)S(1)} %collective-permute-done.38), channel_id=1, source_target_pairs={{0,2},{2,0},{4,6},{6,4},{1,3},{3,1},{5,7},{7,5},{8,10},{10,8},{12,... | collective-permute-start | bytes 786440 | tf_op jit(solution)/shard_map/ppermute | solution.py:351
  98.9 11.4 %collective-permute-start.32 = (f32[64,384]{1,0:T(8,128)S(1)}, f32[64,384]{1,0:T(8,128)S(1)}, u32[]{:S(2)}, u32[]{:S(2)}) collective-permute-start(f32[64,384]{1,0:T(8,128)S(1)} %get-tuple-element.63.a_10_), channel_id=1, source_target_pairs={{0,6},{2,4},{4,2},{6,0},{1,7},{3,5},{5,3},{7,1},{8,14},{10,12},{12... | collective-permute-start | bytes 294920 | tf_op jit(solution)/shard_map/ppermute | solution.py:351
  102.5 8.7 %collective-permute-start.31 = (f32[64,384]{1,0:T(8,128)S(1)}, f32[64,384]{1,0:T(8,128)S(1)}, u32[]{:S(2)}, u32[]{:S(2)}) collective-permute-start(f32[64,384]{1,0:T(8,128)S(1)} %get-tuple-element.63.a_10_), channel_id=1, source_target_pairs={{0,4},{2,6},{4,0},{6,2},{1,5},{3,7},{5,1},{7,3},{8,12},{10,14},{12... | collective-permute-start | bytes 294920 | tf_op jit(solution)/shard_map/ppermute | solution.py:351
  110.4 9.5 %collective-permute-start.24 = (bf16[256,384]{1,0:T(8,128)(2,1)S(1)}, bf16[256,384]{1,0:T(8,128)(2,1)S(1)}, u32[]{:S(2)}, u32[]{:S(2)}) collective-permute-start(bf16[256,384]{1,0:T(8,128)(2,1)S(1)} %get-tuple-element.61.a_2_), channel_id=1, source_target_pairs={{0,4},{2,6},{4,0},{6,2},{1,5},{3,7},{5,1},{7,3},{8,12},{10,14},{12... | collective-permute-start | bytes 589832 | tf_op jit(solution)/shard_map/ppermute | solution.py:351
  111.3 9.4 %collective-permute-start.23 = (bf16[256,384]{1,0:T(8,128)(2,1)S(1)}, bf16[256,384]{1,0:T(8,128)(2,1)S(1)}, u32[]{:S(2)}, u32[]{:S(2)}) collective-permute-start(bf16[256,384]{1,0:T(8,128)(2,1)S(1)} %get-tuple-element.61.a_2_), channel_id=1, source_target_pairs={{0,2},{2,0},{4,6},{6,4},{1,3},{3,1},{5,7},{7,5},{8,10},{10,8},{12,... | collective-permute-start | bytes 589832 | tf_op jit(solution)/shard_map/ppermute | solution.py:351
  112.3 13.1 %collective-permute-start.44 = (f16[256,512]{1,0:T(8,128)(2,1)S(1)}, f16[256,512]{1,0:T(8,128)(2,1)S(1)}, u32[]{:S(2)}, u32[]{:S(2)}) collective-permute-start(f16[256,512]{1,0:T(8,128)(2,1)S(1)} %pad_maximum_fusion.1), channel_id=1, source_target_pairs={{0,2},{2,0},{4,6},{6,4},{1,3},{3,1},{5,7},{7,5},{8,10},{10,8},{12,... | collective-permute-start | bytes 786440 | tf_op jit(solution)/shard_map/ppermute | solution.py:351
  113.3 12.2 %collective-permute-start.43 = (f16[256,512]{1,0:T(8,128)(2,1)S(1)}, f16[256,512]{1,0:T(8,128)(2,1)S(1)}, u32[]{:S(2)}, u32[]{:S(2)}) collective-permute-start(f16[256,512]{1,0:T(8,128)(2,1)S(1)} %pad_maximum_fusion), channel_id=1, source_target_pairs={{0,4},{2,6},{4,0},{6,2},{1,5},{3,7},{5,1},{7,3},{8,12},{10,14},{12... | collective-permute-start | bytes 786440 | tf_op jit(solution)/shard_map/ppermute | solution.py:351
  (35 other events, 381.0 us)

commit v2 on v1

--- a/solution.py
+++ b/solution.py
@@ -164,11 +164,14 @@
     return jnp.concatenate([packed, jnp.zeros_like(packed)], axis=0).astype(bf16)
 
 
+def pairwise(terms):
+    while len(terms) > 1:
+        terms = [a + b for a, b in zip(terms[::2], terms[1::2])]
+    return terms[0]
+
+
 def add_totals(tails):
-    acc = tails[0].astype(f32)
-    for tail in tails[1:]:
-        acc = acc + tail.astype(f32)
-    return jnp.sum(acc, axis=0, keepdims=True)
+    return jnp.sum(pairwise([tail.astype(f32) for tail in tails]), axis=0, keepdims=True)
 
 
 def moment_kernel(nf, block_q, place, *refs):
@@ -209,18 +212,16 @@
 def step_kernel(nf, nr, block_q, count, place, left, *rest):
     halves, totals, lows, rest = rest[:nr], rest[nr : 2 * nr], rest[2 * nr : 3 * nr], rest[3 * nr :]
     codes, near, rest = rest[: nr - 1], rest[nr - 1], rest[nr:]
-    first_q, second_q, first_o, second_o, weight_q, weight_o = rest[:6]
-    copy_q, copy_o, new_q, new_o, step_q, step_o, new_fq, new_sq, new_fo, new_so, table, scale_out = rest[6:18]
-    made_q, made_o, fresh_q, fresh_o, moved_q, moved_o, got_q, got_o, made_fq, made_sq, made_fo, made_so, sems = rest[18:]
+    first_q, second_q, first_o, second_o, weight_q, weight_o, sent_q, sent_o = rest[:8]
+    copy_q, copy_o, new_q, new_o, step_q, step_o, new_fq, new_sq, new_fo, new_so, table, scale_out = rest[8:20]
+    made_q, made_o, fresh_q, fresh_o, moved_q, moved_o, got_q, got_o, made_fq, made_sq, made_fo, made_so, sems = rest[20:]
     f, r = place[0], place[1]
     rows_q, cols_q = weight_q.shape
     rows_o, cols_o = weight_o.shape
     part_q, part_o = rows_q // nr, rows_o // nr
     cut = nf * rows_q
     block_o = cols_o // nr
-    total = totals[0][...]
-    for x in totals[1:]:
-        total = total + x[...]
+    total = pairwise([x[...] for x in totals])
     scale = lax.rsqrt(total / count + mean_eps)
     scale_out[...] = scale
     scale = scale[0:1, 0:1]
@@ -245,7 +246,7 @@
         if mz == 0:
             moved_q[...] = found_q
             fresh_q[...] = weight_q[...] - learn_rate * found_q
-            made_q[at_q, :] = fresh_q[...].astype(bf16)
+            made_q[at_q, :] = (sent_q[...] - learn_rate * found_q).astype(bf16)
             send(moved_q, step_q)
             send(fresh_q, new_q)
             send(made_q.at[at_q, :], copy_q.at[at_q, :])
@@ -261,7 +262,7 @@
         if mz == 0:
             moved_o[...] = found_o
             fresh_o[...] = weight_o[...] - learn_rate * found_o
-            made_o[at_o, :] = fresh_o[...].astype(bf16)
+            made_o[at_o, :] = (sent_o[...] - learn_rate * found_o).astype(bf16)
             send(moved_o, step_o)
             send(fresh_o, new_o)
             send(made_o.at[at_o, :], copy_o.at[at_o, :])
@@ -395,6 +396,8 @@
     code_far = {1: swap(code, "fs", 1, nf)}
     code_far |= {m: swap(code, "fs", m, nf) for m in range(2, nf)}
 
+    sent = [lax.reduce_precision(x * code_scale, 5, 10) * (1.0 / code_scale) for x in (weight_query, weight_output)]
+
     cots = call(
         lambda *a: cot_kernel(nr, *a),
         [shape((tokens, block), bf16)] * nr,
@@ -481,7 +484,7 @@
             shape((rank, cols_q + cols_o), bf16),
             shape((8, 128)),
         ],
-        in_specs=[SMEM] + [VMEM] * (4 * nr + 7),
+        in_specs=[SMEM] + [VMEM] * (4 * nr + 9),
         out_specs=[ANY] * 10 + [VMEM] * 2,
         scratch_shapes=[
             pltpu.VMEM((rows_q * nf, cols_q), bf16),
@@ -498,7 +501,7 @@
         ],
         name="step",
         compiler_params=pltpu.CompilerParams(vmem_limit_bytes=24 * MIB),
-    )(place, left, *halves, *totals, *lows, *codes, decode(corners[1]), *moments, weight_query, weight_output)
+    )(place, left, *halves, *totals, *lows, *codes, decode(corners[1]), *moments, weight_query, weight_output, *sent)
     tops, ends = hold((tops, ends, scale))[:2]
     copy_q, copy_o = pl.pallas_call(
         lambda *a: corner_kernel(nf, nr, *a),

time: 127 us -> 137 us (1.079)
  local copies, waits for them, and re-layouts: 4.92 us -> 10.3 us
  waiting for transfers between devices: 56.1 us -> 57.8 us
    unnamed x28 -> x40, local copies, waits for them, and re-layouts: 3.83 us -> 9.44 us
    ppermute x45, waiting for transfers between devices: 56.1 us -> 57.8 us  [swap(): return lax.ppermute(x, axis, [(i, i ^ m) for i in range(n)])]
  transfers between devices with their start and end apart: 45 -> 45, of which waited for: 15 -> 18; matrix products, arithmetic and copies ran while one was open for 2% -> 2% of each run, Pallas kernels for 8% -> 7%
where the time goes in v2:
time: 137 us
  waiting for transfers between devices  57.8 us (42%)
  starting transfers between devices  51.2 us (37%)
  Pallas kernels  14 us (10%)
  local copies, waits for them, and re-layouts  10.3 us (8%)
  other arithmetic  2.33 us (2%)
    ppermute x45, waiting for transfers between devices, swap(): return lax.ppermute(x, axis, [(i, i ^ m) for i in range(n)])  57.8 us
    ppermute x45, starting transfers between devices, swap(): return lax.ppermute(x, axis, [(i, i ^ m) for i in range(n)])  51.2 us
    unnamed x40, local copies, waits for them, and re-layouts  9.44 us
    pallas_call x8, Pallas kernels, call(): pl.pallas_call(kernel, out_shape=outs, in_specs=[SMEM] + [source] * (len(...  7.57 us
    pallas_call x1, Pallas kernels, local_short(): pl.pallas_call(lambda *a: step_kernel(nf, nr, block_q, count, *a), out_sh...  4.75 us
  transfers between devices with their start and end apart: 45, of which 18 were waited for; matrix products, arithmetic and copies ran while one was open for 2% of the time, Pallas kernels for 7%

profile of v2, /device:TPU:0, one launch (start us, length us, event | category | flops | bytes accessed | tf_op | source)
XLA Modules:
  0.0 136.5 jit_solution(10643351434035022181)
XLA Ops:
  3.2 3.1 %collective-permute-start = (bf16[384,128]{1,0:T(8,128)(2,1)S(1)}, bf16[384,128]{1,0:T(8,128)(2,1)S(1)}, u32[]{:S(2)}, u32[]{:S(2)}) collective-permute-start(bf16[384,128]{1,0:T(8,128)(2,1)S(1)} %get-tuple-element.48), channel_id=1, source_target_pairs={{0,8},{8,0},{16,24},{24,16},{1,9},{9,1},{17,25},{25,17},{2,10},{10... | collective-permute-start | bytes 294920 | tf_op jit(solution)/shard_map/ppermute | solution.py:352
  6.4 2.5 %collective-permute-start.2 = (bf16[192,128]{1,0:T(8,128)(2,1)S(1)}, bf16[192,128]{1,0:T(8,128)(2,1)S(1)}, u32[]{:S(2)}, u32[]{:S(2)}) collective-permute-start(bf16[192,128]{1,0:T(8,128)(2,1)S(1)} %get-tuple-element.49), channel_id=1, source_target_pairs={{0,24},{8,16},{16,8},{24,0},{1,25},{9,17},{17,9},{25,1},{2,26},{10... | collective-permute-start | bytes 147464 | tf_op jit(solution)/shard_map/ppermute | solution.py:352
  9.2 3.9 %collective-permute-done.2 = bf16[192,128]{1,0:T(8,128)(2,1)S(1)} collective-permute-done((bf16[192,128]{1,0:T(8,128)(2,1)S(1)}, bf16[192,128]{1,0:T(8,128)(2,1)S(1)}, u32[]{:S(2)}, u32[]{:S(2)}) %collective-permute-start.2) | collective-permute-done | bytes 49184 | tf_op jit(solution)/shard_map/ppermute | solution.py:352
  14.4 1.6 %collective-permute-start.4 = (bf16[576,128]{1,0:T(8,128)(2,1)S(1)}, bf16[576,128]{1,0:T(8,128)(2,1)S(1)}, u32[]{:S(2)}, u32[]{:S(2)}) collective-permute-start(bf16[576,128]{1,0:T(8,128)(2,1)S(1)} %pad_maximum_fusion.2.a_5_), channel_id=1, source_target_pairs={{0,4},{2,6},{4,0},{6,2},{1,5},{3,7},{5,1},{7,3},{8,12},{10,14},{12... | collective-permute-start | bytes 442376 | tf_op jit(solution)/shard_map/ppermute | solution.py:352
  18.0 5.0 %collective-permute-done.5.a_8_ = bf16[384,128]{1,0:T(8,128)(2,1)S(1)} collective-permute-done((bf16[384,128]{1,0:T(8,128)(2,1)S(1)}, bf16[384,128]{1,0:T(8,128)(2,1)S(1)}, u32[]{:S(2)}, u32[]{:S(2)}) %collective-permute-start.5) | collective-permute-done | bytes 98336 | tf_op jit(solution)/shard_map/ppermute | solution.py:352
  27.9 1.7 %collective-permute-start.12 = (f32[256,128]{1,0:T(8,128)S(1)}, f32[256,128]{1,0:T(8,128)S(1)}, u32[]{:S(2)}, u32[]{:S(2)}) collective-permute-start(f32[256,128]{1,0:T(8,128)S(1)} %get-tuple-element.55.a_5_), channel_id=1, source_target_pairs={{0,6},{2,4},{4,2},{6,0},{1,7},{3,5},{5,3},{7,1},{8,14},{10,12},{12... | collective-permute-start | bytes 393224 | tf_op jit(solution)/shard_map/ppermute | solution.py:352
  36.4 2.6 %collective-permute-done.7.a_2_ = bf16[128,384]{1,0:T(8,128)(2,1)S(1)} collective-permute-done((bf16[128,384]{1,0:T(8,128)(2,1)}, bf16[128,384]{1,0:T(8,128)(2,1)S(1)}, u32[]{:S(2)}, u32[]{:S(2)}) %collective-permute-start.7) | collective-permute-done | bytes 98336 | tf_op jit(solution)/shard_map/ppermute | solution.py:352
  41.4 1.6 %collective-permute-start.9 = (bf16[128,384]{1,0:T(8,128)(2,1)}, bf16[128,384]{1,0:T(8,128)(2,1)S(1)}, u32[]{:S(2)}, u32[]{:S(2)}) collective-permute-start(bf16[128,384]{1,0:T(8,128)(2,1)} %copy-done.18), channel_id=1, source_target_pairs={{0,6},{2,4},{4,2},{6,0},{1,7},{3,5},{5,3},{7,1},{8,14},{10,12},{12... | collective-permute-start | bytes 294920 | tf_op jit(solution)/shard_map/ppermute | solution.py:352
  43.1 4.2 %collective-permute-done.9.a_4_ = bf16[128,384]{1,0:T(8,128)(2,1)S(1)} collective-permute-done((bf16[128,384]{1,0:T(8,128)(2,1)}, bf16[128,384]{1,0:T(8,128)(2,1)S(1)}, u32[]{:S(2)}, u32[]{:S(2)}) %collective-permute-start.9) | collective-permute-done | bytes 98336 | tf_op jit(solution)/shard_map/ppermute | solution.py:352
  49.1 1.7 %shard_map.199 = (f32[64,384]{1,0:T(8,128)S(1)}, f32[64,384]{1,0:T(8,128)S(1)}, f32[64,384]{1,0:T(8,128)S(1)}, f32[64,384]{1,0:T(8,128)S(1)}) custom-call(s32[3]{0:T(128)S(1)} %pad_add_fusion.a_0_.place, bf16[128,384]{1,0:T(8,128)(2,1)S(1)} %copy-done.15, bf16[128,384]{1,0:T(8,128)(2,1)S(1)} %copy-done.17, bf16[128,384]{1,0:T(8,128)(2,1)} %collective-permute-done.8.a_3_, ...), custom_call_target="tpu_custom_call" | custom-call | tf_op jit(solution)/shard_map/pallas_call | solution.py:336
  51.1 2.2 %collective-permute-start.38 = (f16[256,512]{1,0:T(8,128)(2,1)S(1)}, f16[256,512]{1,0:T(8,128)(2,1)S(1)}, u32[]{:S(2)}, u32[]{:S(2)}) collective-permute-start(f16[256,512]{1,0:T(8,128)(2,1)S(1)} %fusion), channel_id=1, source_target_pairs={{0,24},{8,16},{16,8},{24,0},{1,25},{9,17},{17,9},{25,1},{2,26},{10... | collective-permute-start | bytes 786440 | tf_op jit(solution)/shard_map/ppermute | solution.py:352
  55.5 1.7 %collective-permute-start.18 = (f32[64,384]{1,0:T(8,128)S(1)}, f32[64,384]{1,0:T(8,128)S(1)}, u32[]{:S(2)}, u32[]{:S(2)}) collective-permute-start(f32[64,384]{1,0:T(8,128)S(1)} %get-tuple-element.58), channel_id=1, source_target_pairs={{0,16},{8,24},{16,0},{24,8},{1,17},{9,25},{17,1},{25,9},{2,18},{10... | collective-permute-start | bytes 294920 | tf_op jit(solution)/shard_map/ppermute | solution.py:352
  57.3 3.5 %collective-permute-done.17.a_2_ = f32[64,384]{1,0:T(8,128)S(1)} collective-permute-done((f32[64,384]{1,0:T(8,128)S(1)}, f32[64,384]{1,0:T(8,128)S(1)}, u32[]{:S(2)}, u32[]{:S(2)}) %collective-permute-start.17) | collective-permute-done | bytes 98336 | tf_op jit(solution)/shard_map/ppermute | solution.py:352
  60.8 2.5 %collective-permute-start.19 = (f32[64,384]{1,0:T(8,128)S(1)}, f32[64,384]{1,0:T(8,128)S(1)}, u32[]{:S(2)}, u32[]{:S(2)}) collective-permute-start(f32[64,384]{1,0:T(8,128)S(1)} %get-tuple-element.59), channel_id=1, source_target_pairs={{0,24},{8,16},{16,8},{24,0},{1,25},{9,17},{17,9},{25,1},{2,26},{10... | collective-permute-start | bytes 294920 | tf_op jit(solution)/shard_map/ppermute | solution.py:352
  64.5 19.3 %collective-permute-done.18.a_3_ = f32[64,384]{1,0:T(8,128)S(1)} collective-permute-done((f32[64,384]{1,0:T(8,128)S(1)}, f32[64,384]{1,0:T(8,128)S(1)}, u32[]{:S(2)}, u32[]{:S(2)}) %collective-permute-start.18) | collective-permute-done | bytes 98336 | tf_op jit(solution)/shard_map/ppermute | solution.py:352
  84.6 2.3 %collective-permute-start.22 = (bf16[80,384]{1,0:T(8,128)(2,1)S(1)}, bf16[80,384]{1,0:T(8,128)(2,1)S(1)}, u32[]{:S(2)}, u32[]{:S(2)}) collective-permute-start(bf16[80,384]{1,0:T(8,128)(2,1)S(1)} %get-tuple-element.60.a_1_), channel_id=1, source_target_pairs={{0,24},{8,16},{16,8},{24,0},{1,25},{9,17},{17,9},{25,1},{2,26},{10... | collective-permute-start | bytes 184328 | tf_op jit(solution)/shard_map/ppermute | solution.py:352
  94.0 3.1 %collective-permute-done.20.a_2_ = bf16[80,384]{1,0:T(8,128)(2,1)S(1)} collective-permute-done((bf16[80,384]{1,0:T(8,128)(2,1)S(1)}, bf16[80,384]{1,0:T(8,128)(2,1)S(1)}, u32[]{:S(2)}, u32[]{:S(2)}) %collective-permute-start.20) | collective-permute-done | bytes 61472 | tf_op jit(solution)/shard_map/ppermute | solution.py:352
  103.2 3.0 %collective-permute-done.41 = f16[256,512]{1,0:T(8,128)(2,1)S(1)} collective-permute-done((f16[256,512]{1,0:T(8,128)(2,1)S(1)}, f16[256,512]{1,0:T(8,128)(2,1)S(1)}, u32[]{:S(2)}, u32[]{:S(2)}) %collective-permute-start.41) | collective-permute-done | bytes 262176 | tf_op jit(solution)/shard_map/ppermute | solution.py:352
  106.2 2.2 %collective-permute-start.29 = (f32[8,128]{1,0:T(8,128)S(1)}, f32[8,128]{1,0:T(8,128)S(1)}, u32[]{:S(2)}, u32[]{:S(2)}) collective-permute-start(f32[8,128]{1,0:T(8,128)S(1)} %add.10.a_6_), channel_id=1, source_target_pairs={{0,6},{2,4},{4,2},{6,0},{1,7},{3,5},{5,3},{7,1},{8,14},{10,12},{12... | collective-permute-start | bytes 12296 | tf_op jit(solution)/shard_map/ppermute | solution.py:352
  116.1 2.8 %collective-permute-done.27.a_7_ = f32[8,128]{1,0:T(8,128)S(1)} collective-permute-done((f32[8,128]{1,0:T(8,128)S(1)}, f32[8,128]{1,0:T(8,128)S(1)}, u32[]{:S(2)}, u32[]{:S(2)}) %collective-permute-start.27) | collective-permute-done | bytes 4128 | tf_op jit(solution)/shard_map/ppermute | solution.py:352
  125.0 2.6 %collective-permute-done.25.a_5_ = bf16[256,384]{1,0:T(8,128)(2,1)S(1)} collective-permute-done((bf16[256,384]{1,0:T(8,128)(2,1)S(1)}, bf16[256,384]{1,0:T(8,128)(2,1)S(1)}, u32[]{:S(2)}, u32[]{:S(2)}) %collective-permute-start.25) | collective-permute-done | bytes 196640 | tf_op jit(solution)/shard_map/ppermute | solution.py:352
  127.6 1.9 %collective-permute-done.24.a_4_ = bf16[256,384]{1,0:T(8,128)(2,1)S(1)} collective-permute-done((bf16[256,384]{1,0:T(8,128)(2,1)S(1)}, bf16[256,384]{1,0:T(8,128)(2,1)S(1)}, u32[]{:S(2)}, u32[]{:S(2)}) %collective-permute-start.24) | collective-permute-done | bytes 196640 | tf_op jit(solution)/shard_map/ppermute | solution.py:352
  130.0 4.8 %step.1 = (bf16[2048,512]{1,0:T(8,128)(2,1)}, bf16[1024,1024]{1,0:T(8,128)(2,1)}, f32[512,512]{1,0:T(8,128)}, f32[256,1024]{1,0:T(8,128)}, f32[512,512]{1,0:T(8,...) custom-call(s32[3]{0:T(128)S(1)} %pad_add_fusion.a_0_.place, ...), custom_call_target="tpu_custom_call" | custom-call | tf_op jit(solution)/shard_map/step/pallas_call | solution.py:473
  134.9 1.6 %corner.1 = (bf16[2048,512]{1,0:T(8,128)(2,1)}, bf16[1024,1024]{1,0:T(8,128)(2,1)}) custom-call(s32[3]{0:T(128)S(1)} %pad_add_fusion.a_0_.place, bf16[3072,256]{1,0:T(8,128)(2,1)S(1)} %shard_map.197.a_1_, bf16[256,1536]{1,0:T(8,128)(2,1)S(1)} %get-tuple-element.78.a_2_, ...), custom_call_target="tpu_custom_call", output_to_operand_aliasing={{0}: (6, {}), {1}: (7, {})} | custom-call | tf_op jit(solution)/shard_map/corner/pallas_call | solution.py:506
  (138 shorter events, 54.1 us)
Async XLA Ops:
  27.9 11.7 %collective-permute-start.12 = (f32[256,128]{1,0:T(8,128)S(1)}, f32[256,128]{1,0:T(8,128)S(1)}, u32[]{:S(2)}, u32[]{:S(2)}) collective-permute-start(f32[256,128]{1,0:T(8,128)S(1)} %get-tuple-element.55.a_5_), channel_id=1, source_target_pairs={{0,6},{2,4},{4,2},{6,0},{1,7},{3,5},{5,3},{7,1},{8,14},{10,12},{12... | collective-permute-start | bytes 393224 | tf_op jit(solution)/shard_map/ppermute | solution.py:352
  29.6 10.5 %collective-permute-start.11 = (f32[256,128]{1,0:T(8,128)S(1)}, f32[256,128]{1,0:T(8,128)S(1)}, u32[]{:S(2)}, u32[]{:S(2)}) collective-permute-start(f32[256,128]{1,0:T(8,128)S(1)} %get-tuple-element.55.a_5_), channel_id=1, source_target_pairs={{0,4},{2,6},{4,0},{6,2},{1,5},{3,7},{5,1},{7,3},{8,12},{10,14},{12... | collective-permute-start | bytes 393224 | tf_op jit(solution)/shard_map/ppermute | solution.py:352
  30.1 10.1 %collective-permute-start.10 = (f32[256,128]{1,0:T(8,128)S(1)}, f32[256,128]{1,0:T(8,128)S(1)}, u32[]{:S(2)}, u32[]{:S(2)}) collective-permute-start(f32[256,128]{1,0:T(8,128)S(1)} %get-tuple-element.55.a_5_), channel_id=1, source_target_pairs={{0,2},{2,0},{4,6},{6,4},{1,3},{3,1},{5,7},{7,5},{8,10},{10,8},{12,... | collective-permute-start | bytes 393224 | tf_op jit(solution)/shard_map/ppermute | solution.py:352
  50.8 9.9 %collective-permute-start.17 = (f32[64,384]{1,0:T(8,128)S(1)}, f32[64,384]{1,0:T(8,128)S(1)}, u32[]{:S(2)}, u32[]{:S(2)}) collective-permute-start(f32[64,384]{1,0:T(8,128)S(1)} %get-tuple-element.57), channel_id=1, source_target_pairs={{0,8},{8,0},{16,24},{24,16},{1,9},{9,1},{17,25},{25,17},{2,10},{10... | collective-permute-start | bytes 294920 | tf_op jit(solution)/shard_map/ppermute | solution.py:352
  51.1 36.7 %collective-permute-start.38 = (f16[256,512]{1,0:T(8,128)(2,1)S(1)}, f16[256,512]{1,0:T(8,128)(2,1)S(1)}, u32[]{:S(2)}, u32[]{:S(2)}) collective-permute-start(f16[256,512]{1,0:T(8,128)(2,1)S(1)} %fusion), channel_id=1, source_target_pairs={{0,24},{8,16},{16,8},{24,0},{1,25},{9,17},{17,9},{25,1},{2,26},{10... | collective-permute-start | bytes 786440 | tf_op jit(solution)/shard_map/ppermute | solution.py:352
  53.3 36.0 %collective-permute-start.37 = (f16[256,512]{1,0:T(8,128)(2,1)S(1)}, f16[256,512]{1,0:T(8,128)(2,1)S(1)}, u32[]{:S(2)}, u32[]{:S(2)}) collective-permute-start(f16[256,512]{1,0:T(8,128)(2,1)S(1)} %fusion), channel_id=1, source_target_pairs={{0,16},{8,24},{16,0},{24,8},{1,17},{9,25},{17,1},{25,9},{2,18},{10... | collective-permute-start | bytes 786440 | tf_op jit(solution)/shard_map/ppermute | solution.py:352
  54.5 34.7 %collective-permute-start.33 = (f16[256,512]{1,0:T(8,128)(2,1)S(1)}, f16[256,512]{1,0:T(8,128)(2,1)S(1)}, u32[]{:S(2)}, u32[]{:S(2)}) collective-permute-start(f16[256,512]{1,0:T(8,128)(2,1)S(1)} %fusion), channel_id=1, source_target_pairs={{0,8},{8,0},{16,24},{24,16},{1,9},{9,1},{17,25},{25,17},{2,10},{10... | collective-permute-start | bytes 786440 | tf_op jit(solution)/shard_map/ppermute | solution.py:352
  55.5 28.3 %collective-permute-start.18 = (f32[64,384]{1,0:T(8,128)S(1)}, f32[64,384]{1,0:T(8,128)S(1)}, u32[]{:S(2)}, u32[]{:S(2)}) collective-permute-start(f32[64,384]{1,0:T(8,128)S(1)} %get-tuple-element.58), channel_id=1, source_target_pairs={{0,16},{8,24},{16,0},{24,8},{1,17},{9,25},{17,1},{25,9},{2,18},{10... | collective-permute-start | bytes 294920 | tf_op jit(solution)/shard_map/ppermute | solution.py:352
  60.8 23.1 %collective-permute-start.19 = (f32[64,384]{1,0:T(8,128)S(1)}, f32[64,384]{1,0:T(8,128)S(1)}, u32[]{:S(2)}, u32[]{:S(2)}) collective-permute-start(f32[64,384]{1,0:T(8,128)S(1)} %get-tuple-element.59), channel_id=1, source_target_pairs={{0,24},{8,16},{16,8},{24,0},{1,25},{9,17},{17,9},{25,1},{2,26},{10... | collective-permute-start | bytes 294920 | tf_op jit(solution)/shard_map/ppermute | solution.py:352
  87.8 11.0 %collective-permute-start.36 = (f16[256,512]{1,0:T(8,128)(2,1)S(1)}, f16[256,512]{1,0:T(8,128)(2,1)S(1)}, u32[]{:S(2)}, u32[]{:S(2)}) collective-permute-start(f16[256,512]{1,0:T(8,128)(2,1)S(1)} %multiply_convert_fusion), channel_id=1, source_target_pairs={{0,8},{8,0},{16,24},{24,16},{1,9},{9,1},{17,25},{25,17},{2,10},{10... | collective-permute-start | bytes 786440 | tf_op jit(solution)/shard_map/ppermute | solution.py:352
  89.2 34.0 %collective-permute-start.6 = (bf16[3072,128]{1,0:T(8,128)(2,1)S(1)}, bf16[3072,128]{1,0:T(8,128)(2,1)S(1)}, u32[]{:S(2)}, u32[]{:S(2)}) collective-permute-start(bf16[3072,128]{1,0:T(8,128)(2,1)S(1)} %get-tuple-element.50.mine), channel_id=1, source_target_pairs={{0,1},{1,0},{2,3},{3,2},{4,5},{5,4},{6,7},{7,6},{8,9},{9,8},{10,11... | collective-permute-start | bytes 2359304 | tf_op jit(solution)/shard_map/ppermute | solution.py:352
  89.2 11.2 %collective-permute-start.35 = (f16[256,512]{1,0:T(8,128)(2,1)S(1)}, f16[256,512]{1,0:T(8,128)(2,1)S(1)}, u32[]{:S(2)}, u32[]{:S(2)}) collective-permute-start(f16[256,512]{1,0:T(8,128)(2,1)S(1)} %collective-permute-done.33), channel_id=1, source_target_pairs={{0,4},{2,6},{4,0},{6,2},{1,5},{3,7},{5,1},{7,3},{8,12},{10,14},{12... | collective-permute-start | bytes 786440 | tf_op jit(solution)/shard_map/ppermute | solution.py:352
  91.4 9.5 %collective-permute-start.34 = (f16[256,512]{1,0:T(8,128)(2,1)S(1)}, f16[256,512]{1,0:T(8,128)(2,1)S(1)}, u32[]{:S(2)}, u32[]{:S(2)}) collective-permute-start(f16[256,512]{1,0:T(8,128)(2,1)S(1)} %collective-permute-done.33), channel_id=1, source_target_pairs={{0,2},{2,0},{4,6},{6,4},{1,3},{3,1},{5,7},{7,5},{8,10},{10,8},{12,... | collective-permute-start | bytes 786440 | tf_op jit(solution)/shard_map/ppermute | solution.py:352
  97.0 9.1 %collective-permute-start.41 = (f16[256,512]{1,0:T(8,128)(2,1)S(1)}, f16[256,512]{1,0:T(8,128)(2,1)S(1)}, u32[]{:S(2)}, u32[]{:S(2)}) collective-permute-start(f16[256,512]{1,0:T(8,128)(2,1)S(1)} %collective-permute-done.37), channel_id=1, source_target_pairs={{0,4},{2,6},{4,0},{6,2},{1,5},{3,7},{5,1},{7,3},{8,12},{10,14},{12... | collective-permute-start | bytes 786440 | tf_op jit(solution)/shard_map/ppermute | solution.py:352
  98.8 12.0 %collective-permute-start.39 = (f16[256,512]{1,0:T(8,128)(2,1)S(1)}, f16[256,512]{1,0:T(8,128)(2,1)S(1)}, u32[]{:S(2)}, u32[]{:S(2)}) collective-permute-start(f16[256,512]{1,0:T(8,128)(2,1)S(1)} %collective-permute-done.37), channel_id=1, source_target_pairs={{0,2},{2,0},{4,6},{6,4},{1,3},{3,1},{5,7},{7,5},{8,10},{10,8},{12,... | collective-permute-start | bytes 786440 | tf_op jit(solution)/shard_map/ppermute | solution.py:352
  100.4 8.8 %collective-permute-start.42 = (f16[256,512]{1,0:T(8,128)(2,1)S(1)}, f16[256,512]{1,0:T(8,128)(2,1)S(1)}, u32[]{:S(2)}, u32[]{:S(2)}) collective-permute-start(f16[256,512]{1,0:T(8,128)(2,1)S(1)} %collective-permute-done.38), channel_id=1, source_target_pairs={{0,4},{2,6},{4,0},{6,2},{1,5},{3,7},{5,1},{7,3},{8,12},{10,14},{12... | collective-permute-start | bytes 786440 | tf_op jit(solution)/shard_map/ppermute | solution.py:352
  102.1 10.3 %collective-permute-start.40 = (f16[256,512]{1,0:T(8,128)(2,1)S(1)}, f16[256,512]{1,0:T(8,128)(2,1)S(1)}, u32[]{:S(2)}, u32[]{:S(2)}) collective-permute-start(f16[256,512]{1,0:T(8,128)(2,1)S(1)} %collective-permute-done.38), channel_id=1, source_target_pairs={{0,2},{2,0},{4,6},{6,4},{1,3},{3,1},{5,7},{7,5},{8,10},{10,8},{12,... | collective-permute-start | bytes 786440 | tf_op jit(solution)/shard_map/ppermute | solution.py:352
  110.8 8.8 %collective-permute-start.32 = (f32[64,384]{1,0:T(8,128)S(1)}, f32[64,384]{1,0:T(8,128)S(1)}, u32[]{:S(2)}, u32[]{:S(2)}) collective-permute-start(f32[64,384]{1,0:T(8,128)S(1)} %get-tuple-element.63.a_10_), channel_id=1, source_target_pairs={{0,6},{2,4},{4,2},{6,0},{1,7},{3,5},{5,3},{7,1},{8,14},{10,12},{12... | collective-permute-start | bytes 294920 | tf_op jit(solution)/shard_map/ppermute | solution.py:352
  112.4 8.8 %collective-permute-start.31 = (f32[64,384]{1,0:T(8,128)S(1)}, f32[64,384]{1,0:T(8,128)S(1)}, u32[]{:S(2)}, u32[]{:S(2)}) collective-permute-start(f32[64,384]{1,0:T(8,128)S(1)} %get-tuple-element.63.a_10_), channel_id=1, source_target_pairs={{0,4},{2,6},{4,0},{6,2},{1,5},{3,7},{5,1},{7,3},{8,12},{10,14},{12... | collective-permute-start | bytes 294920 | tf_op jit(solution)/shard_map/ppermute | solution.py:352
  119.0 8.7 %collective-permute-start.25 = (bf16[256,384]{1,0:T(8,128)(2,1)S(1)}, bf16[256,384]{1,0:T(8,128)(2,1)S(1)}, u32[]{:S(2)}, u32[]{:S(2)}) collective-permute-start(bf16[256,384]{1,0:T(8,128)(2,1)S(1)} %get-tuple-element.61.a_2_), channel_id=1, source_target_pairs={{0,6},{2,4},{4,2},{6,0},{1,7},{3,5},{5,3},{7,1},{8,14},{10,12},{12... | collective-permute-start | bytes 589832 | tf_op jit(solution)/shard_map/ppermute | solution.py:352
  119.6 9.9 %collective-permute-start.24 = (bf16[256,384]{1,0:T(8,128)(2,1)S(1)}, bf16[256,384]{1,0:T(8,128)(2,1)S(1)}, u32[]{:S(2)}, u32[]{:S(2)}) collective-permute-start(bf16[256,384]{1,0:T(8,128)(2,1)S(1)} %get-tuple-element.61.a_2_), channel_id=1, source_target_pairs={{0,4},{2,6},{4,0},{6,2},{1,5},{3,7},{5,1},{7,3},{8,12},{10,14},{12... | collective-permute-start | bytes 589832 | tf_op jit(solution)/shard_map/ppermute | solution.py:352
  121.2 8.8 %collective-permute-start.23 = (bf16[256,384]{1,0:T(8,128)(2,1)S(1)}, bf16[256,384]{1,0:T(8,128)(2,1)S(1)}, u32[]{:S(2)}, u32[]{:S(2)}) collective-permute-start(bf16[256,384]{1,0:T(8,128)(2,1)S(1)} %get-tuple-element.61.a_2_), channel_id=1, source_target_pairs={{0,2},{2,0},{4,6},{6,4},{1,3},{3,1},{5,7},{7,5},{8,10},{10,8},{12,... | collective-permute-start | bytes 589832 | tf_op jit(solution)/shard_map/ppermute | solution.py:352
  122.5 12.3 %collective-permute-start.44 = (f16[256,512]{1,0:T(8,128)(2,1)S(1)}, f16[256,512]{1,0:T(8,128)(2,1)S(1)}, u32[]{:S(2)}, u32[]{:S(2)}) collective-permute-start(f16[256,512]{1,0:T(8,128)(2,1)S(1)} %pad_maximum_fusion.1), channel_id=1, source_target_pairs={{0,2},{2,0},{4,6},{6,4},{1,3},{3,1},{5,7},{7,5},{8,10},{10,8},{12,... | collective-permute-start | bytes 786440 | tf_op jit(solution)/shard_map/ppermute | solution.py:352
  123.2 11.5 %collective-permute-start.43 = (f16[256,512]{1,0:T(8,128)(2,1)S(1)}, f16[256,512]{1,0:T(8,128)(2,1)S(1)}, u32[]{:S(2)}, u32[]{:S(2)}) collective-permute-start(f16[256,512]{1,0:T(8,128)(2,1)S(1)} %pad_maximum_fusion), channel_id=1, source_target_pairs={{0,4},{2,6},{4,0},{6,2},{1,5},{3,7},{5,1},{7,3},{8,12},{10,14},{12... | collective-permute-start | bytes 786440 | tf_op jit(solution)/shard_map/ppermute | solution.py:352
  (41 other events, 310.6 us)
